TPU v7x, 32 devices: a whole 2x2x4 slice. The times are simulated.
32 devices in a mesh: ep: 16 (over z, y, x), tp: 2 (over core).
Axes of the slice: x: 2, y: 2, z: 4, core: 2. Of those that a mesh axis runs over, the one named last changes fastest.
Arguments:
- tokens: bfloat16 [8192, 2048], P(('ep', 'tp')), may hold values from -6 to 6
- norm_gain: float32 [2048], replicated, may hold values from 0.1 to 1.9
- expert_ids: int32 [8192, 2], P(('ep', 'tp')), may hold values from 0 to 15, all different within a row; in each aligned block of 256 rows (0 to 255, 256 to 511, ...) at most 48 rows name the same one
- route_weights: float32 [8192, 2], P(('ep', 'tp')), may hold values from 0.2 to 1.2
- expert_gate: bfloat16 [16, 2048, 512], P('ep', None, 'tp'), may hold values from -0.125 to 0.125
- expert_up: bfloat16 [16, 2048, 512], P('ep', None, 'tp'), may hold values from -0.125 to 0.125
- expert_down: bfloat16 [16, 512, 2048], P('ep', 'tp'), may hold values from -0.25 to 0.25
- shared_gate: bfloat16 [2048, 512], P(None, 'tp'), may hold values from -0.125 to 0.125
- shared_up: bfloat16 [2048, 512], P(None, 'tp'), may hold values from -0.125 to 0.125
- shared_down: bfloat16 [512, 2048], P('tp'), may hold values from -0.25 to 0.25
Outputs:
- mixed: bfloat16 [8192, 2048], P(('ep', 'tp'))
Inputs may be any that keep to these rules, and one draw needn't show every extreme that they name: `expert_ids`: each token names 2 different experts. Among the tokens of one device (aligned blocks of 256 rows) no expert is named by more than 48 tokens, and in every block some expert is named by exactly 48.
All inputs are finite; a program needn't handle non-finite values.
Results may differ from a plain program's by a relative error of at most 0.0075.
Values may be sent and summed in bfloat16 or wider, within the bound.
No kernel may reach another device: no remote copies, remote signals or barrier semaphores. Data moves between devices by JAX's collectives and lax.ppermute only.
A program may use at most 64 MiB of HBM per device.

v0:
```python
import functools
import math

import jax
import jax.numpy as jnp
from jax import lax
from jax.experimental import pallas as pl
from jax.experimental.pallas import tpu as pltpu
from jax.sharding import PartitionSpec as P


epsilon = 1e-06
SPLIT = 12
SPARE = 6 * 1024 * 1024
BF16, F32 = jnp.bfloat16, jnp.float32


def dot(left, right):
    return jnp.dot(left, right, preferred_element_type=F32)


def call(kernel, outs, *args, lazy=0, scratch=(), flops=0):
    total, count = len(args), len(args) + len(outs)
    scalars = [a.dtype == jnp.int32 for a in args]
    moved = sum(a.size * a.dtype.itemsize for a in args)
    moved += sum(o.size * jnp.dtype(o.dtype).itemsize for o in outs)

    def wrapped(*refs):
        held, rest, sems = refs[:count], refs[count:-1], refs[-1]
        local = list(held)
        copies = {}
        for i in range(count):
            if i >= total or not scalars[i]:
                local[i], rest = rest[0], rest[1:]
            if i < total and not scalars[i]:
                copies[i] = pltpu.make_async_copy(held[i], local[i], sems.at[i])
                copies[i].start()
        for i in range(total - lazy):
            if i in copies:
                copies[i].wait()
        waits = [copies[i].wait for i in range(total - lazy, total)]
        kernel(*(waits and [waits]), *local, *rest)
        backs = [
            pltpu.make_async_copy(local[i], held[i], sems.at[i]) for i in range(total, count)
        ]
        for back in backs:
            back.start()
        for back in backs:
            back.wait()

    anywhere = pl.BlockSpec(memory_space=pltpu.HBM)
    in_specs = [pl.BlockSpec(memory_space=pltpu.SMEM) if s else anywhere for s in scalars]
    buffers = [pltpu.VMEM(a.shape, a.dtype) for a, s in zip(args, scalars) if not s]
    buffers += [pltpu.VMEM(o.shape, o.dtype) for o in outs]
    grant = SPARE + moved + sum(math.prod(b.shape) * b.dtype.itemsize for b in scratch)
    return pl.pallas_call(
        wrapped,
        out_shape=tuple([pltpu.HBM(o.shape, o.dtype) for o in outs]),
        in_specs=in_specs,
        out_specs=tuple([anywhere] * len(outs)),
        scratch_shapes=buffers + list(scratch) + [pltpu.SemaphoreType.DMA((count,))],
        compiler_params=pltpu.CompilerParams(vmem_limit_bytes=grant),
        cost_estimate=pl.CostEstimate(flops=flops, bytes_accessed=moved, transcendentals=0),
    )(
        *[
            a if s else pltpu.with_memory_space_constraint(a, pltpu.HBM)
            for a, s in zip(args, scalars)
        ]
    )


def array(shape, dtype=BF16):
    return jax.ShapeDtypeStruct(shape, dtype)


def norm_kernel(tokens_ref, gain_ref, normed_ref, *first_refs):
    values = tokens_ref[...].astype(F32)
    factor = lax.rsqrt(jnp.mean(values * values, axis=1, keepdims=True) + epsilon)
    normed = (values * factor * gain_ref[...]).astype(BF16)
    normed_ref[...] = normed
    for i, ref in enumerate(first_refs):
        ref[...] = normed[:, i * ref.shape[1] : (i + 1) * ref.shape[1]]


def ranks(member, axis):
    rows = member.shape[axis]
    one = lax.broadcasted_iota(jnp.int32, (rows, rows), 0)
    two = lax.broadcasted_iota(jnp.int32, (rows, rows), 1)
    flat = jnp.where(member, 1.0, 0.0).astype(BF16)
    if axis:
        count = dot(flat, jnp.where(one < two, 1.0, 0.0).astype(BF16))
    else:
        count = dot(jnp.where(two < one, 1.0, 0.0).astype(BF16), flat)
    return jnp.where(member, count, -1.0)


def slots_of(experts, cap, axis):
    shape = (experts * cap, experts) if axis == 0 else (experts, experts * cap)
    start = lax.broadcasted_iota(jnp.int32, shape, 1 - axis) * cap
    place = lax.broadcasted_iota(jnp.int32, shape, axis) - start
    inside = (place >= 0) & (place < cap)
    number = jnp.sum(jnp.where(inside, place, 0).astype(F32), axis=1 - axis, keepdims=True)
    return jnp.where(inside, 1.0, 0.0).astype(BF16), number


def picks(packet, me, experts, cap):
    numbers = (lax.broadcasted_iota(jnp.int32, (experts, 1), 0) ^ me).astype(F32)
    expand, place = slots_of(experts, cap, 0)
    member = (packet[0:1, :] == numbers) | (packet[1:2, :] == numbers)
    spread = dot(expand, ranks(member, 1).astype(BF16))
    return jnp.where(spread == place, 1.0, 0.0).astype(BF16)


def weighted(packet, me, experts, cap):
    rows = packet.shape[1]
    columns = jnp.concatenate([packet, jnp.zeros((128 - packet.shape[0], rows), F32)]).T
    numbers = (lax.broadcasted_iota(jnp.int32, (1, experts), 1) ^ me).astype(F32)
    expand, place = slots_of(experts, cap, 1)
    one, two = columns[:, 0:1] == numbers, columns[:, 1:2] == numbers
    spread = dot(ranks(one | two, 0).astype(BF16), expand)
    weight = jnp.where(one, columns[:, 2:3], 0.0) + jnp.where(two, columns[:, 3:4], 0.0)
    high = weight.astype(BF16)
    low = (weight - high.astype(F32)).astype(BF16)
    chosen = spread == place
    return [jnp.where(chosen, dot(part, expand), 0.0).astype(BF16) for part in (high, low)]


def put(refs, rows):
    size = refs[0].shape[0]
    for i, ref in enumerate(refs):
        ref[...] = rows[i * size : (i + 1) * size, :]


def gather(refs, into, row=0, column=0):
    size = refs[0].shape[0]
    for i, ref in enumerate(refs):
        start = row + i * size
        into[start : start + size, column : column + ref.shape[1]] = ref[...]


def put_all(ref, me, first, rows):
    if len(ref.shape) == 2:
        ref[first : first + rows.shape[0], :] = rows
        return
    size = ref.shape[1]
    for i in range(rows.shape[0] // size):
        ref[me ^ (first // size + i)] = rows[i * size : (i + 1) * size, :]


def gather_all(ref, me, first, into, columns):
    total = into.shape[0]
    if len(ref.shape) == 2:
        into[:, columns] = ref[first : first + total, :]
        return
    size = ref.shape[1]
    for i in range(total // size):
        into[i * size : (i + 1) * size, columns] = ref[me ^ (first // size + i)]


def send_kernel(experts, cap, me_ref, packet_ref, normed_ref, *outs):
    pick = picks(packet_ref[...], me_ref[0], experts, cap)
    near = experts // 2 * cap
    segments, plain_ref = outs[:-1], outs[-1]
    width = segments[0].shape[1]
    put(segments, dot(pick[:near], normed_ref[:, :width]).astype(BF16))
    put_all(plain_ref, me_ref[0], 0, dot(pick, normed_ref[:, width:]).astype(BF16))


def other_kernel(experts, cap, me_ref, packet_ref, block_ref, *outs):
    pick = picks(packet_ref[...], me_ref[0], experts, cap)
    put(outs, dot(pick, block_ref[...]).astype(BF16))


def ffn_kernel(count, waits, me_ref, *refs):
    near_in, refs = refs[:count], refs[count:]
    far_in, refs = (refs[:count], refs[count : 2 * count]), refs[2 * count :]
    plain_ref, weights, refs = refs[0], refs[1:7], refs[7:]
    near_out, far_out, refs = refs[:count], refs[count : 2 * count], refs[2 * count :]
    back_ref, rows_ref = refs
    near, model_width = rows_ref.shape[0] // 2, rows_ref.shape[1]
    width = near_in[0].shape[1]
    gather(near_in, rows_ref)
    for i, segments in enumerate(far_in):
        gather(segments, rows_ref, near, i * segments[0].shape[1])
    gather_all(plain_ref, me_ref[0], 0, rows_ref, slice(width, model_width))
    hidden = []
    for gate, up in ((0, 1), (2, 3)):
        waits[gate]()
        waits[up]()
        value = dot(rows_ref[...], weights[gate][...])
        value = value / (1.0 + jnp.exp(-value)) * dot(rows_ref[...], weights[up][...])
        hidden.append(value.astype(BF16))
    waits[4]()
    waits[5]()

    def down(rows, columns):
        return sum(dot(h[rows], weights[4 + i][:, columns]) for i, h in enumerate(hidden))

    for half, targets in enumerate((near_out, far_out)):
        rows = slice(half * near, (half + 1) * near)
        put(targets, down(rows, slice(0, width)).astype(BF16))
        rest = down(rows, slice(width, model_width)).astype(BF16)
        put_all(back_ref, me_ref[0], half * near, rest)


def partial_kernel(count, experts, cap, me_ref, packet_ref, *refs):
    masks = weighted(packet_ref[...], me_ref[0], experts, cap)
    segments, out_ref, rows_ref = refs[:count], refs[count], refs[count + 1]
    gather(segments, rows_ref)
    out_ref[...] = sum(dot(mask, rows_ref[...]) for mask in masks).astype(BF16)


def shared_kernel(waits, normed_ref, *refs):
    weights, out_ref = refs[:6], refs[6]
    normed = normed_ref[...]
    total = 0.0
    for gate, up, down in ((0, 1, 4), (2, 3, 5)):
        for w in (gate, up, down):
            waits[w]()
        value = dot(normed, weights[gate][...])
        hidden = value / (1.0 + jnp.exp(-value)) * dot(normed, weights[up][...])
        total = total + dot(hidden.astype(BF16), weights[down][...])
    out_ref[...] = total


def mine_kernel(count, experts, cap, me_ref, packet_ref, *refs):
    masks = weighted(packet_ref[...], me_ref[0], experts, cap)
    near = experts // 2 * cap
    segments, back_ref, shared_ref, out_ref, near_rows, all_rows = (
        refs[:count],
        *refs[count:],
    )
    gather(segments, near_rows)
    gather_all(back_ref, me_ref[0], 0, all_rows, slice(0, all_rows.shape[1]))
    split = near_rows.shape[1]
    one = sum(dot(mask[:, :near], near_rows[...]) for mask in masks)
    two = sum(dot(mask, all_rows[...]) for mask in masks)
    out_ref[:, :split] = shared_ref[:, :split] + one
    out_ref[:, split:] = shared_ref[:, split:] + two


def last_kernel(mine_ref, passed_ref, out_ref):
    split = passed_ref.shape[1]
    out_ref[:, :split] = (mine_ref[:, :split] + passed_ref[...].astype(F32)).astype(BF16)
    out_ref[:, split:] = mine_ref[:, split:].astype(BF16)


def swap_cores(array):
    size = lax.axis_size("tp")
    return lax.ppermute(array, "tp", [(i, (i + 1) % size) for i in range(size)])


def swap(array, bits):
    size = lax.axis_size("ep")
    return lax.ppermute(array, "ep", [(i, i ^ bits) for i in range(size)])


def exchange(segments):
    if len(segments) > 1:
        return [swap(segment, i) if i else segment for i, segment in enumerate(segments)]
    size = lax.axis_size("ep")
    half = size // 2
    rows = segments[0]
    order = jnp.arange(half) ^ (lax.axis_index("ep") % half)
    groups = [list(range(half)), list(range(half, size))]
    blocks = rows.reshape(half, rows.shape[0] // half, rows.shape[1])[order]
    blocks = lax.all_to_all(blocks, "ep", 0, 0, tiled=True, axis_index_groups=groups)
    return [blocks[order].reshape(rows.shape)]


def exchange_all(rows):
    size = lax.axis_size("ep")
    order = jnp.arange(size) ^ lax.axis_index("ep")
    flat = len(rows.shape) == 2
    blocks = rows.reshape(size, rows.shape[0] // size, rows.shape[1])[order] if flat else rows
    blocks = lax.all_to_all(blocks, "ep", 0, 0, tiled=True)
    return blocks[order].reshape(rows.shape) if flat else blocks


def body(
    tokens,
    norm_gain,
    expert_ids,
    route_weights,
    expert_gate,
    expert_up,
    expert_down,
    shared_gate,
    shared_up,
    shared_down,
):
    return layer(
        tokens,
        norm_gain,
        expert_ids,
        route_weights,
        (expert_gate[0], expert_up[0], expert_down[0]),
        (shared_gate, shared_up, shared_down),
    )


def both_halves(gate_w, up_w, down_w):
    gate_o, up_o = swap_cores(gate_w), swap_cores(up_w)
    return gate_w, up_w, gate_o, up_o, down_w, swap_cores(down_w)


def layer(tokens, norm_gain, expert_ids, route_weights, routed_w, shared_w):
    rows, model_width = tokens.shape
    ep_size = lax.axis_size("ep")
    half = ep_size // 2
    cap = 3 * rows * expert_ids.shape[1] // (2 * ep_size)
    width = model_width * SPLIT // 16
    rest = model_width - width
    near = half * cap
    count = half if half <= 8 else 1
    part = near // count
    hidden = 2 * routed_w[0].shape[1]

    me = lax.axis_index("ep").astype(jnp.int32)[None]
    plain_shape = (ep_size, cap, rest) if count > 1 else (ep_size * cap, rest)

    normed, *first = call(
        norm_kernel,
        [array((rows, model_width))] + [array((rows, width // 2))] * 2,
        tokens,
        norm_gain[None, :],
        flops=4 * rows * model_width,
    )
    mirrored = [swap(block, half) for block in first]
    packet = jnp.concatenate([expert_ids.T.astype(F32), route_weights.T])
    other_packet = swap(packet, half)
    *own, plain = call(
        functools.partial(send_kernel, ep_size, cap),
        [array((part, width))] * count + [array(plain_shape)],
        me,
        packet,
        normed,
        flops=2 * near * rows * (model_width + rest),
    )
    own_in = exchange(own)
    plain_in = exchange_all(plain)
    weights = both_halves(*routed_w)
    shared = both_halves(*shared_w)

    other_in = []
    for block in mirrored:
        other = call(
            functools.partial(other_kernel, half, cap),
            [array((part, width // 2))] * count,
            me,
            other_packet,
            block,
            flops=near * rows * width,
        )
        other_in += exchange(other)
    *done, plain_out = call(
        functools.partial(ffn_kernel, count),
        [array((part, width))] * (2 * count) + [array(plain_shape)],
        me,
        *own_in,
        *other_in,
        plain_in,
        *weights,
        lazy=6,
        scratch=[pltpu.VMEM((2 * near, model_width), BF16)],
        flops=12 * near * model_width * hidden,
    )
    plain_back = exchange_all(plain_out)
    other_back = exchange(done[count:])
    own_back = exchange(done[:count])
    (partial,) = call(
        functools.partial(partial_kernel, count, half, cap),
        [array((rows, width))],
        me,
        other_packet,
        *other_back,
        scratch=[pltpu.VMEM((near, width), BF16)],
        flops=4 * near * rows * width,
    )
    passed = swap(partial, half)
    (shared_out,) = call(
        shared_kernel,
        [array((rows, model_width), F32)],
        normed,
        *shared,
        lazy=6,
        flops=6 * rows * model_width * hidden,
    )
    (mine,) = call(
        functools.partial(mine_kernel, count, ep_size, cap),
        [array((rows, model_width), F32)],
        me,
        packet,
        *own_back,
        plain_back,
        shared_out,
        scratch=[pltpu.VMEM((near, width), BF16), pltpu.VMEM((2 * near, rest), BF16)],
        flops=4 * near * rows * (model_width + rest),
    )
    (out,) = call(last_kernel, [array((rows, model_width))], mine, passed, flops=rows * model_width)
    return out


def solution(mesh):
    placed = (
        P(("ep", "tp"), None),
        P(),
        P(("ep", "tp"), None),
        P(("ep", "tp"), None),
        P("ep", None, "tp"),
        P("ep", None, "tp"),
        P("ep", "tp", None),
        P(None, "tp"),
        P(None, "tp"),
        P("tp", None),
    )
    return jax.shard_map(
        body, mesh=mesh, in_specs=placed, out_specs=P(("ep", "tp"), None), check_vma=False
    )
```

profile of v0, /device:TPU:4, one launch (start us, length us, event | category | flops | bytes accessed | tf_op | source)
XLA Modules:
  0.0 213.2 jit_solution(9575236949444822582)
XLA Ops:
  0.7 3.0 %shard_map.100 = (bf16[256,2048]{1,0:T(8,128)(2,1)}, bf16[256,768]{1,0:T(8,128)(2,1)}, bf16[256,768]{1,0:T(8,128)(2,1)}) custom-call(bf16[256,2048]{1,0:T(8,128)(2,1)} %refs_0_.1, f32[1,2048]{1,0:T(1,128)} %bitcast.8), custom_call_target="tpu_custom_call" | custom-call | flops 2097152 | bytes 2891776 | tf_op jit(solution)/shard_map/pallas_call | solution.py:56
  5.1 3.5 %shard_map.101 = (bf16[48,1536]{1,0:T(8,128)(2,1)}, bf16[48,1536]{1,0:T(8,128)(2,1)}, bf16[48,1536]{1,0:T(8,128)(2,1)}, bf16[48,1536]{1,0:T(8,128)(2,1)}, bf16[4...) custom-call(s32[1]{0:T(128)} %bitcast.refs_0_, ...), custom_call_target="tpu_custom_call" | custom-call | flops 503316480 | bytes 3018756 | tf_op jit(solution)/shard_map/pallas_call | solution.py:56
  8.6 7.3 %all-to-all-start = ((bf16[16,48,512]{2,1,0:T(8,128)(2,1)}), bf16[16,48,512]{2,1,0:T(8,128)(2,1)S(1)}, u32[]{:S(2)}, u32[]{:S(2)}) async-start(bf16[16,48,512]{2,1,0:T(8,128)(2,1)} %get-tuple-element.77), calls=%async_computation | async-start | bytes 1572864 | tf_op jit(solution)/shard_map/all_to_all | solution.py:276
  23.2 12.4 %collective-permute-done.7.refs_1_ = f32[4,256]{1,0:T(4,128)S(1)} collective-permute-done((f32[4,256]{1,0:T(4,128)S(1)}, f32[4,256]{1,0:T(4,128)S(1)}, u32[]{:S(2)}, u32[]{:S(2)}) %collective-permute-start.7) | collective-permute-done | bytes 4128 | tf_op jit(solution)/shard_map/ppermute | solution.py:255
  35.7 2.9 %collective-permute-start.8 = (bf16[256,768]{1,0:T(8,128)(2,1)S(1)}, bf16[256,768]{1,0:T(8,128)(2,1)S(1)}, u32[]{:S(2)}, u32[]{:S(2)}) collective-permute-start(bf16[256,768]{1,0:T(8,128)(2,1)S(1)} %copy-done.19), channel_id=1, source_target_pairs={{0,16},{2,18},{4,20},{6,22},{8,24},{10,26},{12,28},{14,30},{16,0},... | collective-permute-start | bytes 1179656 | tf_op jit(solution)/shard_map/ppermute | solution.py:255
  39.3 5.7 %collective-permute-done.4.refs_6_ = bf16[48,1536]{1,0:T(8,128)(2,1)S(1)} collective-permute-done((bf16[48,1536]{1,0:T(8,128)(2,1)}, bf16[48,1536]{1,0:T(8,128)(2,1)S(1)}, u32[]{:S(2)}, u32[]{:S(2)}) %collective-permute-start.4) | collective-permute-done | bytes 147488 | tf_op jit(solution)/shard_map/ppermute | solution.py:255
  45.0 5.3 %collective-permute-done.5.refs_7_ = bf16[48,1536]{1,0:T(8,128)(2,1)S(1)} collective-permute-done((bf16[48,1536]{1,0:T(8,128)(2,1)}, bf16[48,1536]{1,0:T(8,128)(2,1)S(1)}, u32[]{:S(2)}, u32[]{:S(2)}) %collective-permute-start.5) | collective-permute-done | bytes 147488 | tf_op jit(solution)/shard_map/ppermute | solution.py:255
  50.9 2.9 %collective-permute-start.16 = (bf16[256,768]{1,0:T(8,128)(2,1)S(1)}, bf16[256,768]{1,0:T(8,128)(2,1)S(1)}, u32[]{:S(2)}, u32[]{:S(2)}) collective-permute-start(bf16[256,768]{1,0:T(8,128)(2,1)S(1)} %copy-done.18), channel_id=1, source_target_pairs={{0,16},{2,18},{4,20},{6,22},{8,24},{10,26},{12,28},{14,30},{16,0},... | collective-permute-start | bytes 1179656 | tf_op jit(solution)/shard_map/ppermute | solution.py:255
  53.8 11.7 %collective-permute-done.8.refs_2_ = bf16[256,768]{1,0:T(8,128)(2,1)S(1)} collective-permute-done((bf16[256,768]{1,0:T(8,128)(2,1)S(1)}, bf16[256,768]{1,0:T(8,128)(2,1)S(1)}, u32[]{:S(2)}, u32[]{:S(2)}) %collective-permute-start.8) | collective-permute-done | bytes 393248 | tf_op jit(solution)/shard_map/ppermute | solution.py:255
  66.2 2.4 %shard_map.102 = (bf16[48,768]{1,0:T(8,128)(2,1)}, bf16[48,768]{1,0:T(8,128)(2,1)}, bf16[48,768]{1,0:T(8,128)(2,1)}, bf16[48,768]{1,0:T(8,128)(2,1)}, bf16[48,76...) custom-call(s32[1]{0:T(128)} %bitcast.refs_0_, ...), custom_call_target="tpu_custom_call" | custom-call | flops 150994944 | bytes 987140 | tf_op jit(solution)/shard_map/pallas_call | solution.py:56
  68.7 5.7 %collective-permute-done.6.refs_8_ = bf16[48,1536]{1,0:T(8,128)(2,1)S(1)} collective-permute-done((bf16[48,1536]{1,0:T(8,128)(2,1)}, bf16[48,1536]{1,0:T(8,128)(2,1)S(1)}, u32[]{:S(2)}, u32[]{:S(2)}) %collective-permute-start.6) | collective-permute-done | bytes 147488 | tf_op jit(solution)/shard_map/ppermute | solution.py:255
  78.9 2.6 %collective-permute-done.11.refs_12_ = bf16[48,768]{1,0:T(8,128)(2,1)S(1)} collective-permute-done((bf16[48,768]{1,0:T(8,128)(2,1)}, bf16[48,768]{1,0:T(8,128)(2,1)S(1)}, u32[]{:S(2)}, u32[]{:S(2)}) %collective-permute-start.11) | collective-permute-done | bytes 73760 | tf_op jit(solution)/shard_map/ppermute | solution.py:255
  87.9 2.4 %shard_map.103 = (bf16[48,768]{1,0:T(8,128)(2,1)}, bf16[48,768]{1,0:T(8,128)(2,1)}, bf16[48,768]{1,0:T(8,128)(2,1)}, bf16[48,768]{1,0:T(8,128)(2,1)}, bf16[48,76...) custom-call(s32[1]{0:T(128)} %bitcast.refs_0_, ...), custom_call_target="tpu_custom_call" | custom-call | flops 150994944 | bytes 987140 | tf_op jit(solution)/shard_map/pallas_call | solution.py:56
  91.4 2.6 %collective-permute-done.15.refs_16_ = bf16[48,768]{1,0:T(8,128)(2,1)S(1)} collective-permute-done((bf16[48,768]{1,0:T(8,128)(2,1)}, bf16[48,768]{1,0:T(8,128)(2,1)S(1)}, u32[]{:S(2)}, u32[]{:S(2)}) %collective-permute-start.15) | collective-permute-done | bytes 73760 | tf_op jit(solution)/shard_map/ppermute | solution.py:255
  95.0 2.5 %collective-permute-start.19 = (bf16[48,768]{1,0:T(8,128)(2,1)}, bf16[48,768]{1,0:T(8,128)(2,1)S(1)}, u32[]{:S(2)}, u32[]{:S(2)}) collective-permute-start(bf16[48,768]{1,0:T(8,128)(2,1)} %get-tuple-element.72), channel_id=1, source_target_pairs={{0,6},{2,4},{4,2},{6,0},{8,14},{10,12},{12,10},{14,8},{16,22},{18,... | collective-permute-start | bytes 221192 | tf_op jit(solution)/shard_map/ppermute | solution.py:255
  105.9 4.6 %collective-permute-start.23 = (bf16[48,768]{1,0:T(8,128)(2,1)}, bf16[48,768]{1,0:T(8,128)(2,1)S(1)}, u32[]{:S(2)}, u32[]{:S(2)}) collective-permute-start(bf16[48,768]{1,0:T(8,128)(2,1)} %get-tuple-element.76), channel_id=1, source_target_pairs={{0,14},{2,12},{4,10},{6,8},{8,6},{10,4},{12,2},{14,0},{16,30},{18,... | collective-permute-start | bytes 221192 | tf_op jit(solution)/shard_map/ppermute | solution.py:255
  118.1 9.8 %shard_map.104 = (bf16[48,1536]{1,0:T(8,128)(2,1)}, bf16[48,1536]{1,0:T(8,128)(2,1)}, bf16[48,1536]{1,0:T(8,128)(2,1)}, bf16[48,1536]{1,0:T(8,128)(2,1)}, bf16[4...) custom-call(s32[1]{0:T(128)} %bitcast.refs_0_, ...), custom_call_target="tpu_custom_call" | custom-call | flops 4831838208 | bytes 12582916 | tf_op jit(solution)/shard_map/pallas_call | solution.py:56
  127.9 5.3 %all-to-all-start.1 = ((bf16[16,48,512]{2,1,0:T(8,128)(2,1)}), bf16[16,48,512]{2,1,0:T(8,128)(2,1)S(1)}, u32[]{:S(2)}, u32[]{:S(2)}) async-start(bf16[16,48,512]{2,1,0:T(8,128)(2,1)} %get-tuple-element.86), calls=%async_computation.1 | async-start | bytes 1572864 | tf_op jit(solution)/shard_map/all_to_all | solution.py:276
  135.8 5.8 %collective-permute-done.37.refs_3_ = bf16[48,1536]{1,0:T(8,128)(2,1)S(1)} collective-permute-done((bf16[48,1536]{1,0:T(8,128)(2,1)}, bf16[48,1536]{1,0:T(8,128)(2,1)S(1)}, u32[]{:S(2)}, u32[]{:S(2)}) %collective-permute-start.37) | collective-permute-done | bytes 147488 | tf_op jit(solution)/shard_map/ppermute | solution.py:255
  142.9 2.4 %collective-permute-start.40 = (bf16[48,1536]{1,0:T(8,128)(2,1)}, bf16[48,1536]{1,0:T(8,128)(2,1)S(1)}, u32[]{:S(2)}, u32[]{:S(2)}) collective-permute-start(bf16[48,1536]{1,0:T(8,128)(2,1)} %get-tuple-element.91), channel_id=1, source_target_pairs={{0,8},{2,10},{4,12},{6,14},{8,0},{10,2},{12,4},{14,6},{16,24},{18,... | collective-permute-start | bytes 442376 | tf_op jit(solution)/shard_map/ppermute | solution.py:255
  145.3 2.6 %collective-permute-done.39.refs_5_ = bf16[48,1536]{1,0:T(8,128)(2,1)S(1)} collective-permute-done((bf16[48,1536]{1,0:T(8,128)(2,1)}, bf16[48,1536]{1,0:T(8,128)(2,1)S(1)}, u32[]{:S(2)}, u32[]{:S(2)}) %collective-permute-start.39) | collective-permute-done | bytes 147488 | tf_op jit(solution)/shard_map/ppermute | solution.py:255
  147.9 2.5 %collective-permute-start.41 = (bf16[48,1536]{1,0:T(8,128)(2,1)}, bf16[48,1536]{1,0:T(8,128)(2,1)S(1)}, u32[]{:S(2)}, u32[]{:S(2)}) collective-permute-start(bf16[48,1536]{1,0:T(8,128)(2,1)} %get-tuple-element.92), channel_id=1, source_target_pairs={{0,10},{2,8},{4,14},{6,12},{8,2},{10,0},{12,6},{14,4},{16,26},{18,... | collective-permute-start | bytes 442376 | tf_op jit(solution)/shard_map/ppermute | solution.py:255
  151.6 3.7 %collective-permute-done.41.refs_7_ = bf16[48,1536]{1,0:T(8,128)(2,1)S(1)} collective-permute-done((bf16[48,1536]{1,0:T(8,128)(2,1)}, bf16[48,1536]{1,0:T(8,128)(2,1)S(1)}, u32[]{:S(2)}, u32[]{:S(2)}) %collective-permute-start.41) | collective-permute-done | bytes 147488 | tf_op jit(solution)/shard_map/ppermute | solution.py:255
  155.3 2.8 %collective-permute-start.43 = (bf16[48,1536]{1,0:T(8,128)(2,1)}, bf16[48,1536]{1,0:T(8,128)(2,1)S(1)}, u32[]{:S(2)}, u32[]{:S(2)}) collective-permute-start(bf16[48,1536]{1,0:T(8,128)(2,1)} %get-tuple-element.94), channel_id=1, source_target_pairs={{0,14},{2,12},{4,10},{6,8},{8,6},{10,4},{12,2},{14,0},{16,30},{18,... | collective-permute-start | bytes 442376 | tf_op jit(solution)/shard_map/ppermute | solution.py:255
  158.1 4.3 %collective-permute-done.43.refs_9_ = bf16[48,1536]{1,0:T(8,128)(2,1)S(1)} collective-permute-done((bf16[48,1536]{1,0:T(8,128)(2,1)}, bf16[48,1536]{1,0:T(8,128)(2,1)S(1)}, u32[]{:S(2)}, u32[]{:S(2)}) %collective-permute-start.43) | collective-permute-done | bytes 147488 | tf_op jit(solution)/shard_map/ppermute | solution.py:255
  163.1 4.0 %shard_map.107 = bf16[256,1536]{1,0:T(8,128)(2,1)} custom-call(s32[1]{0:T(128)} %bitcast.refs_0_, f32[4,256]{1,0:T(4,128)} %copy-done.57, bf16[48,1536]{1,0:T(8,128)(2,1)} %get-tuple-element.87.refs_2_, bf16[48,1536]{1,0:T(8,128)(2,1)} %copy-done.36, bf16[48,1536]{1,0:T(8,128)(2,1)} %copy-done.37, bf16[48,1536]{1,0:T(8,128)(2,1)} %copy-done.38, ...), custom_call_target="tpu_custom_call" | custom-call | flops 603979776 | bytes 1970180 | tf_op jit(solution)/shard_map/pallas_call | solution.py:56
  167.1 2.7 %collective-permute-start.44 = (bf16[256,1536]{1,0:T(8,128)(2,1)}, bf16[256,1536]{1,0:T(8,128)(2,1)}, u32[]{:S(2)}, u32[]{:S(2)}) collective-permute-start(bf16[256,1536]{1,0:T(8,128)(2,1)} %shard_map.107), channel_id=1, source_target_pairs={{0,16},{2,18},{4,20},{6,22},{8,24},{10,26},{12,28},{14,30},{16,0},... | collective-permute-start | bytes 2359304 | tf_op jit(solution)/shard_map/ppermute | solution.py:255
  179.6 4.7 %collective-permute-start.33 = (bf16[48,1536]{1,0:T(8,128)(2,1)S(1)}, bf16[48,1536]{1,0:T(8,128)(2,1)S(1)}, u32[]{:S(2)}, u32[]{:S(2)}) collective-permute-start(bf16[48,1536]{1,0:T(8,128)(2,1)S(1)} %copy-done.29), channel_id=1, source_target_pairs={{0,14},{2,12},{4,10},{6,8},{8,6},{10,4},{12,2},{14,0},{16,30},{18,... | collective-permute-start | bytes 442376 | tf_op jit(solution)/shard_map/ppermute | solution.py:255
  184.2 6.4 %shard_map.105.refs_11_ = f32[256,2048]{1,0:T(8,128)} custom-call(bf16[256,2048]{1,0:T(8,128)(2,1)} %get-tuple-element.50.refs_2_.refs_0_, bf16[2048,256]{1,0:T(8,128)(2,1)} %refs_1_.1, bf16[2048,256]{1,0:T(8,128)(2,1)} %refs_2_.1, bf16[2048,256]{1,0:T(8,128)(2,1)} %copy-done.3, bf16[2048,256]{1,0:T(8,128)(2,1)} %copy-done.4, bf16[256,2048]{1,0:T(8,128)(2,1)} %refs_5_.1, ...), custom_call_target="tpu_custom_call" | custom-call | flops 1610612736 | bytes 9437184 | tf_op jit(solution)/shard_map/pallas_call | solution.py:56
  194.9 8.3 %collective-permute-done.33.refs_9_ = bf16[48,1536]{1,0:T(8,128)(2,1)S(1)} collective-permute-done((bf16[48,1536]{1,0:T(8,128)(2,1)S(1)}, bf16[48,1536]{1,0:T(8,128)(2,1)S(1)}, u32[]{:S(2)}, u32[]{:S(2)}) %collective-permute-start.33) | collective-permute-done | bytes 147488 | tf_op jit(solution)/shard_map/ppermute | solution.py:255
  204.1 6.0 %shard_map.106.refs_0_ = f32[256,2048]{1,0:T(8,128)} custom-call(s32[1]{0:T(128)} %bitcast.refs_0_, f32[4,256]{1,0:T(4,128)} %pad_maximum_fusion.refs_1_, bf16[48,1536]{1,0:T(8,128)(2,1)} %get-tuple-element.78.refs_2_, bf16[48,1536]{1,0:T(8,128)(2,1)} %copy-done.7, bf16[48,1536]{1,0:T(8,128)(2,1)} %copy-done.8, bf16[48,1536]{1,0:T(8,128)(2,1)} %copy-done.9, ...), custom_call_target="tpu_custom_call" | custom-call | flops 1006632960 | bytes 6164484 | tf_op jit(solution)/shard_map/pallas_call | solution.py:56
  210.2 2.9 %shard_map.108 = bf16[256,2048]{1,0:T(8,128)(2,1)} custom-call(f32[256,2048]{1,0:T(8,128)} %shard_map.106.refs_0_, bf16[256,1536]{1,0:T(8,128)(2,1)} %collective-permute-done.44.refs_1_), custom_call_target="tpu_custom_call" | custom-call | flops 524288 | bytes 3932160 | tf_op jit(solution)/shard_map/pallas_call | solution.py:56
  (189 shorter events, 60.7 us)
Async XLA Ops:
  8.6 108.5 %all-to-all-start = ((bf16[16,48,512]{2,1,0:T(8,128)(2,1)}), bf16[16,48,512]{2,1,0:T(8,128)(2,1)S(1)}, u32[]{:S(2)}, u32[]{:S(2)}) async-start(bf16[16,48,512]{2,1,0:T(8,128)(2,1)} %get-tuple-element.77), calls=%async_computation | async-start | bytes 1572864 | tf_op jit(solution)/shard_map/all_to_all | solution.py:276
  15.9 19.8 %collective-permute-start = (bf16[48,1536]{1,0:T(8,128)(2,1)}, bf16[48,1536]{1,0:T(8,128)(2,1)S(1)}, u32[]{:S(2)}, u32[]{:S(2)}) collective-permute-start(bf16[48,1536]{1,0:T(8,128)(2,1)} %get-tuple-element.52), channel_id=1, source_target_pairs={{0,2},{2,0},{4,6},{6,4},{8,10},{10,8},{12,14},{14,12},{16,18},{18,... | collective-permute-start | bytes 442376 | tf_op jit(solution)/shard_map/ppermute | solution.py:255
  17.4 21.3 %collective-permute-start.1 = (bf16[48,1536]{1,0:T(8,128)(2,1)}, bf16[48,1536]{1,0:T(8,128)(2,1)S(1)}, u32[]{:S(2)}, u32[]{:S(2)}) collective-permute-start(bf16[48,1536]{1,0:T(8,128)(2,1)} %get-tuple-element.53), channel_id=1, source_target_pairs={{0,4},{2,6},{4,0},{6,2},{8,12},{10,14},{12,8},{14,10},{16,20},{18,... | collective-permute-start | bytes 442376 | tf_op jit(solution)/shard_map/ppermute | solution.py:255
  17.9 17.7 %collective-permute-start.7 = (f32[4,256]{1,0:T(4,128)S(1)}, f32[4,256]{1,0:T(4,128)S(1)}, u32[]{:S(2)}, u32[]{:S(2)}) collective-permute-start(f32[4,256]{1,0:T(4,128)S(1)} %copy-done.14), channel_id=1, source_target_pairs={{0,16},{2,18},{4,20},{6,22},{8,24},{10,26},{12,28},{14,30},{16,0},... | collective-permute-start | bytes 12296 | tf_op jit(solution)/shard_map/ppermute | solution.py:255
  20.3 18.5 %collective-permute-start.2 = (bf16[48,1536]{1,0:T(8,128)(2,1)}, bf16[48,1536]{1,0:T(8,128)(2,1)S(1)}, u32[]{:S(2)}, u32[]{:S(2)}) collective-permute-start(bf16[48,1536]{1,0:T(8,128)(2,1)} %get-tuple-element.54), channel_id=1, source_target_pairs={{0,6},{2,4},{4,2},{6,0},{8,14},{10,12},{12,10},{14,8},{16,22},{18,... | collective-permute-start | bytes 442376 | tf_op jit(solution)/shard_map/ppermute | solution.py:255
  21.7 17.1 %collective-permute-start.3 = (bf16[48,1536]{1,0:T(8,128)(2,1)}, bf16[48,1536]{1,0:T(8,128)(2,1)S(1)}, u32[]{:S(2)}, u32[]{:S(2)}) collective-permute-start(bf16[48,1536]{1,0:T(8,128)(2,1)} %get-tuple-element.55), channel_id=1, source_target_pairs={{0,8},{2,10},{4,12},{6,14},{8,0},{10,2},{12,4},{14,6},{16,24},{18,... | collective-permute-start | bytes 442376 | tf_op jit(solution)/shard_map/ppermute | solution.py:255
  35.7 9.3 %collective-permute-start.4 = (bf16[48,1536]{1,0:T(8,128)(2,1)}, bf16[48,1536]{1,0:T(8,128)(2,1)S(1)}, u32[]{:S(2)}, u32[]{:S(2)}) collective-permute-start(bf16[48,1536]{1,0:T(8,128)(2,1)} %get-tuple-element.56), channel_id=1, source_target_pairs={{0,10},{2,8},{4,14},{6,12},{8,2},{10,0},{12,6},{14,4},{16,26},{18,... | collective-permute-start | bytes 442376 | tf_op jit(solution)/shard_map/ppermute | solution.py:255
  35.7 29.8 %collective-permute-start.8 = (bf16[256,768]{1,0:T(8,128)(2,1)S(1)}, bf16[256,768]{1,0:T(8,128)(2,1)S(1)}, u32[]{:S(2)}, u32[]{:S(2)}) collective-permute-start(bf16[256,768]{1,0:T(8,128)(2,1)S(1)} %copy-done.19), channel_id=1, source_target_pairs={{0,16},{2,18},{4,20},{6,22},{8,24},{10,26},{12,28},{14,30},{16,0},... | collective-permute-start | bytes 1179656 | tf_op jit(solution)/shard_map/ppermute | solution.py:255
  38.6 11.7 %collective-permute-start.5 = (bf16[48,1536]{1,0:T(8,128)(2,1)}, bf16[48,1536]{1,0:T(8,128)(2,1)S(1)}, u32[]{:S(2)}, u32[]{:S(2)}) collective-permute-start(bf16[48,1536]{1,0:T(8,128)(2,1)} %get-tuple-element.57), channel_id=1, source_target_pairs={{0,12},{2,14},{4,8},{6,10},{8,4},{10,6},{12,0},{14,2},{16,28},{18,... | collective-permute-start | bytes 442376 | tf_op jit(solution)/shard_map/ppermute | solution.py:255
  38.8 76.3 %collective-permute-start.24 = (bf16[2048,256]{1,0:T(8,128)(2,1)S(1)}, bf16[2048,256]{1,0:T(8,128)(2,1)S(1)}, u32[]{:S(2)}, u32[]{:S(2)}) collective-permute-start(bf16[2048,256]{1,0:T(8,128)(2,1)S(1)} %bitcast.11), channel_id=1, source_target_pairs={{0,1},{1,0},{2,3},{3,2},{4,5},{5,4},{6,7},{7,6},{8,9},{9,8},{10,11... | collective-permute-start | bytes 3145736 | tf_op jit(solution)/shard_map/ppermute | solution.py:250
  38.9 76.2 %collective-permute-start.25 = (bf16[2048,256]{1,0:T(8,128)(2,1)}, bf16[2048,256]{1,0:T(8,128)(2,1)S(1)}, u32[]{:S(2)}, u32[]{:S(2)}) collective-permute-start(bf16[2048,256]{1,0:T(8,128)(2,1)} %bitcast.12), channel_id=1, source_target_pairs={{0,1},{1,0},{2,3},{3,2},{4,5},{5,4},{6,7},{7,6},{8,9},{9,8},{10,11... | collective-permute-start | bytes 3145736 | tf_op jit(solution)/shard_map/ppermute | solution.py:250
  45.0 72.1 %collective-permute-start.26 = (bf16[256,2048]{1,0:T(8,128)(2,1)}, bf16[256,2048]{1,0:T(8,128)(2,1)}, u32[]{:S(2)}, u32[]{:S(2)}) collective-permute-start(bf16[256,2048]{1,0:T(8,128)(2,1)} %bitcast.14), channel_id=1, source_target_pairs={{0,1},{1,0},{2,3},{3,2},{4,5},{5,4},{6,7},{7,6},{8,9},{9,8},{10,11... | collective-permute-start | bytes 3145736 | tf_op jit(solution)/shard_map/ppermute | solution.py:250
  50.9 25.0 %collective-permute-start.16 = (bf16[256,768]{1,0:T(8,128)(2,1)S(1)}, bf16[256,768]{1,0:T(8,128)(2,1)S(1)}, u32[]{:S(2)}, u32[]{:S(2)}) collective-permute-start(bf16[256,768]{1,0:T(8,128)(2,1)S(1)} %copy-done.18), channel_id=1, source_target_pairs={{0,16},{2,18},{4,20},{6,22},{8,24},{10,26},{12,28},{14,30},{16,0},... | collective-permute-start | bytes 1179656 | tf_op jit(solution)/shard_map/ppermute | solution.py:255
  65.5 8.9 %collective-permute-start.6 = (bf16[48,1536]{1,0:T(8,128)(2,1)}, bf16[48,1536]{1,0:T(8,128)(2,1)S(1)}, u32[]{:S(2)}, u32[]{:S(2)}) collective-permute-start(bf16[48,1536]{1,0:T(8,128)(2,1)} %get-tuple-element.58), channel_id=1, source_target_pairs={{0,14},{2,12},{4,10},{6,8},{8,6},{10,4},{12,2},{14,0},{16,30},{18,... | collective-permute-start | bytes 442376 | tf_op jit(solution)/shard_map/ppermute | solution.py:255
  87.2 6.9 %collective-permute-start.15 = (bf16[48,768]{1,0:T(8,128)(2,1)}, bf16[48,768]{1,0:T(8,128)(2,1)S(1)}, u32[]{:S(2)}, u32[]{:S(2)}) collective-permute-start(bf16[48,768]{1,0:T(8,128)(2,1)} %get-tuple-element.67), channel_id=1, source_target_pairs={{0,14},{2,12},{4,10},{6,8},{8,6},{10,4},{12,2},{14,0},{16,30},{18,... | collective-permute-start | bytes 221192 | tf_op jit(solution)/shard_map/ppermute | solution.py:255
  105.9 7.1 %collective-permute-start.23 = (bf16[48,768]{1,0:T(8,128)(2,1)}, bf16[48,768]{1,0:T(8,128)(2,1)S(1)}, u32[]{:S(2)}, u32[]{:S(2)}) collective-permute-start(bf16[48,768]{1,0:T(8,128)(2,1)} %get-tuple-element.76), channel_id=1, source_target_pairs={{0,14},{2,12},{4,10},{6,8},{8,6},{10,4},{12,2},{14,0},{16,30},{18,... | collective-permute-start | bytes 221192 | tf_op jit(solution)/shard_map/ppermute | solution.py:255
  127.9 75.3 %all-to-all-start.1 = ((bf16[16,48,512]{2,1,0:T(8,128)(2,1)}), bf16[16,48,512]{2,1,0:T(8,128)(2,1)S(1)}, u32[]{:S(2)}, u32[]{:S(2)}) async-start(bf16[16,48,512]{2,1,0:T(8,128)(2,1)} %get-tuple-element.86), calls=%async_computation.1 | async-start | bytes 1572864 | tf_op jit(solution)/shard_map/all_to_all | solution.py:276
  133.2 36.9 %collective-permute-start.34 = (bf16[2048,256]{1,0:T(8,128)(2,1)S(1)}, bf16[2048,256]{1,0:T(8,128)(2,1)S(1)}, u32[]{:S(2)}, u32[]{:S(2)}) collective-permute-start(bf16[2048,256]{1,0:T(8,128)(2,1)S(1)} %copy-done.1), channel_id=1, source_target_pairs={{0,1},{1,0},{2,3},{3,2},{4,5},{5,4},{6,7},{7,6},{8,9},{9,8},{10,11... | collective-permute-start | bytes 3145736 | tf_op jit(solution)/shard_map/ppermute | solution.py:250
  133.3 38.0 %collective-permute-start.35 = (bf16[2048,256]{1,0:T(8,128)(2,1)S(1)}, bf16[2048,256]{1,0:T(8,128)(2,1)S(1)}, u32[]{:S(2)}, u32[]{:S(2)}) collective-permute-start(bf16[2048,256]{1,0:T(8,128)(2,1)S(1)} %copy-done.2), channel_id=1, source_target_pairs={{0,1},{1,0},{2,3},{3,2},{4,5},{5,4},{6,7},{7,6},{8,9},{9,8},{10,11... | collective-permute-start | bytes 3145736 | tf_op jit(solution)/shard_map/ppermute | solution.py:250
  133.8 7.9 %collective-permute-start.37 = (bf16[48,1536]{1,0:T(8,128)(2,1)}, bf16[48,1536]{1,0:T(8,128)(2,1)S(1)}, u32[]{:S(2)}, u32[]{:S(2)}) collective-permute-start(bf16[48,1536]{1,0:T(8,128)(2,1)} %get-tuple-element.88), channel_id=1, source_target_pairs={{0,2},{2,0},{4,6},{6,4},{8,10},{10,8},{12,14},{14,12},{16,18},{18,... | collective-permute-start | bytes 442376 | tf_op jit(solution)/shard_map/ppermute | solution.py:255
  135.3 38.2 %collective-permute-start.36 = (bf16[256,2048]{1,0:T(8,128)(2,1)}, bf16[256,2048]{1,0:T(8,128)(2,1)S(1)}, u32[]{:S(2)}, u32[]{:S(2)}) collective-permute-start(bf16[256,2048]{1,0:T(8,128)(2,1)} %refs_5_.1), channel_id=1, source_target_pairs={{0,1},{1,0},{2,3},{3,2},{4,5},{5,4},{6,7},{7,6},{8,9},{9,8},{10,11... | collective-permute-start | bytes 3145736 | tf_op jit(solution)/shard_map/ppermute | solution.py:250
  135.3 7.6 %collective-permute-start.38 = (bf16[48,1536]{1,0:T(8,128)(2,1)}, bf16[48,1536]{1,0:T(8,128)(2,1)S(1)}, u32[]{:S(2)}, u32[]{:S(2)}) collective-permute-start(bf16[48,1536]{1,0:T(8,128)(2,1)} %get-tuple-element.89), channel_id=1, source_target_pairs={{0,4},{2,6},{4,0},{6,2},{8,12},{10,14},{12,8},{14,10},{16,20},{18,... | collective-permute-start | bytes 442376 | tf_op jit(solution)/shard_map/ppermute | solution.py:255
  142.9 7.5 %collective-permute-start.40 = (bf16[48,1536]{1,0:T(8,128)(2,1)}, bf16[48,1536]{1,0:T(8,128)(2,1)S(1)}, u32[]{:S(2)}, u32[]{:S(2)}) collective-permute-start(bf16[48,1536]{1,0:T(8,128)(2,1)} %get-tuple-element.91), channel_id=1, source_target_pairs={{0,8},{2,10},{4,12},{6,14},{8,0},{10,2},{12,4},{14,6},{16,24},{18,... | collective-permute-start | bytes 442376 | tf_op jit(solution)/shard_map/ppermute | solution.py:255
  147.9 7.3 %collective-permute-start.41 = (bf16[48,1536]{1,0:T(8,128)(2,1)}, bf16[48,1536]{1,0:T(8,128)(2,1)S(1)}, u32[]{:S(2)}, u32[]{:S(2)}) collective-permute-start(bf16[48,1536]{1,0:T(8,128)(2,1)} %get-tuple-element.92), channel_id=1, source_target_pairs={{0,10},{2,8},{4,14},{6,12},{8,2},{10,0},{12,6},{14,4},{16,26},{18,... | collective-permute-start | bytes 442376 | tf_op jit(solution)/shard_map/ppermute | solution.py:255
  150.4 7.7 %collective-permute-start.42 = (bf16[48,1536]{1,0:T(8,128)(2,1)}, bf16[48,1536]{1,0:T(8,128)(2,1)S(1)}, u32[]{:S(2)}, u32[]{:S(2)}) collective-permute-start(bf16[48,1536]{1,0:T(8,128)(2,1)} %get-tuple-element.93), channel_id=1, source_target_pairs={{0,12},{2,14},{4,8},{6,10},{8,4},{10,6},{12,0},{14,2},{16,28},{18,... | collective-permute-start | bytes 442376 | tf_op jit(solution)/shard_map/ppermute | solution.py:255
  155.3 7.2 %collective-permute-start.43 = (bf16[48,1536]{1,0:T(8,128)(2,1)}, bf16[48,1536]{1,0:T(8,128)(2,1)S(1)}, u32[]{:S(2)}, u32[]{:S(2)}) collective-permute-start(bf16[48,1536]{1,0:T(8,128)(2,1)} %get-tuple-element.94), channel_id=1, source_target_pairs={{0,14},{2,12},{4,10},{6,8},{8,6},{10,4},{12,2},{14,0},{16,30},{18,... | collective-permute-start | bytes 442376 | tf_op jit(solution)/shard_map/ppermute | solution.py:255
  167.1 43.0 %collective-permute-start.44 = (bf16[256,1536]{1,0:T(8,128)(2,1)}, bf16[256,1536]{1,0:T(8,128)(2,1)}, u32[]{:S(2)}, u32[]{:S(2)}) collective-permute-start(bf16[256,1536]{1,0:T(8,128)(2,1)} %shard_map.107), channel_id=1, source_target_pairs={{0,16},{2,18},{4,20},{6,22},{8,24},{10,26},{12,28},{14,30},{16,0},... | collective-permute-start | bytes 2359304 | tf_op jit(solution)/shard_map/ppermute | solution.py:255
  171.3 8.2 %collective-permute-start.29 = (bf16[48,1536]{1,0:T(8,128)(2,1)S(1)}, bf16[48,1536]{1,0:T(8,128)(2,1)S(1)}, u32[]{:S(2)}, u32[]{:S(2)}) collective-permute-start(bf16[48,1536]{1,0:T(8,128)(2,1)S(1)} %copy-done.33), channel_id=1, source_target_pairs={{0,6},{2,4},{4,2},{6,0},{8,14},{10,12},{12,10},{14,8},{16,22},{18,... | collective-permute-start | bytes 442376 | tf_op jit(solution)/shard_map/ppermute | solution.py:255
  173.5 17.7 %collective-permute-start.30 = (bf16[48,1536]{1,0:T(8,128)(2,1)S(1)}, bf16[48,1536]{1,0:T(8,128)(2,1)S(1)}, u32[]{:S(2)}, u32[]{:S(2)}) collective-permute-start(bf16[48,1536]{1,0:T(8,128)(2,1)S(1)} %copy-done.32), channel_id=1, source_target_pairs={{0,8},{2,10},{4,12},{6,14},{8,0},{10,2},{12,4},{14,6},{16,24},{18,... | collective-permute-start | bytes 442376 | tf_op jit(solution)/shard_map/ppermute | solution.py:255
  176.5 16.8 %collective-permute-start.31 = (bf16[48,1536]{1,0:T(8,128)(2,1)S(1)}, bf16[48,1536]{1,0:T(8,128)(2,1)S(1)}, u32[]{:S(2)}, u32[]{:S(2)}) collective-permute-start(bf16[48,1536]{1,0:T(8,128)(2,1)S(1)} %copy-done.31), channel_id=1, source_target_pairs={{0,10},{2,8},{4,14},{6,12},{8,2},{10,0},{12,6},{14,4},{16,26},{18,... | collective-permute-start | bytes 442376 | tf_op jit(solution)/shard_map/ppermute | solution.py:255
  176.6 18.3 %collective-permute-start.32 = (bf16[48,1536]{1,0:T(8,128)(2,1)S(1)}, bf16[48,1536]{1,0:T(8,128)(2,1)S(1)}, u32[]{:S(2)}, u32[]{:S(2)}) collective-permute-start(bf16[48,1536]{1,0:T(8,128)(2,1)S(1)} %copy-done.30), channel_id=1, source_target_pairs={{0,12},{2,14},{4,8},{6,10},{8,4},{10,6},{12,0},{14,2},{16,28},{18,... | collective-permute-start | bytes 442376 | tf_op jit(solution)/shard_map/ppermute | solution.py:255
  179.6 23.6 %collective-permute-start.33 = (bf16[48,1536]{1,0:T(8,128)(2,1)S(1)}, bf16[48,1536]{1,0:T(8,128)(2,1)S(1)}, u32[]{:S(2)}, u32[]{:S(2)}) collective-permute-start(bf16[48,1536]{1,0:T(8,128)(2,1)S(1)} %copy-done.29), channel_id=1, source_target_pairs={{0,14},{2,12},{4,10},{6,8},{8,6},{10,4},{12,2},{14,0},{16,30},{18,... | collective-permute-start | bytes 442376 | tf_op jit(solution)/shard_map/ppermute | solution.py:255
  (73 other events, 1494.8 us)
where the time goes:
time: 214 us; the launch traced here: 213 us
  waiting for transfers between devices  93.2 us (44%)
  starting transfers between devices  70.9 us (33%)
  Pallas kernels  40.5 us (19%)
  local copies, waits for them, and re-layouts  5.92 us (3%)
    ppermute x39, waiting for transfers between devices, swap(): return lax.ppermute(array, 'ep', [(i, i ^ bits) for i in range(size)])  93.1 us
    ppermute x39, starting transfers between devices, swap(): return lax.ppermute(array, 'ep', [(i, i ^ bits) for i in range(size)])  57.2 us
    pallas_call x9, Pallas kernels, call(): pl.pallas_call(wrapped, out_shape=tuple([pltpu.HBM(o.shape, o.dtype) for...  40.5 us
    all_to_all x2, starting transfers between devices, exchange_all(): blocks = lax.all_to_all(blocks, 'ep', 0, 0, tiled=True)  12.6 us
    unnamed x116, local copies, waits for them, and re-layouts  5.92 us
  transfers between devices with their start and end apart: 47, of which 28 were waited for; matrix products, arithmetic and copies ran while one was open for 0% of the time, Pallas kernels for 10%

commit v1 on v0

--- a/solution.py
+++ b/solution.py
@@ -19,9 +19,11 @@
     return jnp.dot(left, right, preferred_element_type=F32)
 
 
-def call(kernel, outs, *args, lazy=0, scratch=(), flops=0):
+def call(kernel, outs, *args, lazy=0, resident=0, keep=0, scratch=(), flops=0):
     total, count = len(args), len(args) + len(outs)
     scalars = [a.dtype == jnp.int32 for a in args]
+    still = [s or i >= total - resident for i, s in enumerate(scalars)]
+    still += [i >= len(outs) - keep for i in range(len(outs))]
     moved = sum(a.size * a.dtype.itemsize for a in args)
     moved += sum(o.size * jnp.dtype(o.dtype).itemsize for o in outs)
 
@@ -30,9 +32,9 @@
         local = list(held)
         copies = {}
         for i in range(count):
-            if i >= total or not scalars[i]:
+            if not still[i]:
                 local[i], rest = rest[0], rest[1:]
-            if i < total and not scalars[i]:
+            if i < total and not still[i]:
                 copies[i] = pltpu.make_async_copy(held[i], local[i], sems.at[i])
                 copies[i].start()
         for i in range(total - lazy):
@@ -41,7 +43,9 @@
         waits = [copies[i].wait for i in range(total - lazy, total)]
         kernel(*(waits and [waits]), *local, *rest)
         backs = [
-            pltpu.make_async_copy(local[i], held[i], sems.at[i]) for i in range(total, count)
+            pltpu.make_async_copy(local[i], held[i], sems.at[i])
+            for i in range(total, count)
+            if not still[i]
         ]
         for back in backs:
             back.start()
@@ -49,24 +53,21 @@
             back.wait()
 
     anywhere = pl.BlockSpec(memory_space=pltpu.HBM)
-    in_specs = [pl.BlockSpec(memory_space=pltpu.SMEM) if s else anywhere for s in scalars]
-    buffers = [pltpu.VMEM(a.shape, a.dtype) for a, s in zip(args, scalars) if not s]
-    buffers += [pltpu.VMEM(o.shape, o.dtype) for o in outs]
+    near, scalar = pl.BlockSpec(memory_space=pltpu.VMEM), pl.BlockSpec(memory_space=pltpu.SMEM)
+    in_specs = [scalar if s else near if t else anywhere for s, t in zip(scalars, still)]
+    buffers = [pltpu.VMEM(a.shape, a.dtype) for a, t in zip(args, still) if not t]
+    buffers += [pltpu.VMEM(o.shape, o.dtype) for o, t in zip(outs, still[total:]) if not t]
+    spaces = [pltpu.VMEM if t else pltpu.HBM for t in still[total:]]
     grant = SPARE + moved + sum(math.prod(b.shape) * b.dtype.itemsize for b in scratch)
     return pl.pallas_call(
         wrapped,
-        out_shape=tuple([pltpu.HBM(o.shape, o.dtype) for o in outs]),
+        out_shape=tuple([space(o.shape, o.dtype) for o, space in zip(outs, spaces)]),
         in_specs=in_specs,
-        out_specs=tuple([anywhere] * len(outs)),
+        out_specs=tuple([near if t else anywhere for t in still[total:]]),
         scratch_shapes=buffers + list(scratch) + [pltpu.SemaphoreType.DMA((count,))],
         compiler_params=pltpu.CompilerParams(vmem_limit_bytes=grant),
         cost_estimate=pl.CostEstimate(flops=flops, bytes_accessed=moved, transcendentals=0),
-    )(
-        *[
-            a if s else pltpu.with_memory_space_constraint(a, pltpu.HBM)
-            for a, s in zip(args, scalars)
-        ]
-    )
+    )(*[a if s else pltpu.with_memory_space_constraint(a, pltpu.HBM) for a, s in zip(args, still)])
 
 
 def array(shape, dtype=BF16):
@@ -194,7 +195,8 @@
     waits[5]()
 
     def down(rows, columns):
-        return sum(dot(h[rows], weights[4 + i][:, columns]) for i, h in enumerate(hidden))
+        left = jnp.concatenate([h[rows] for h in hidden], axis=1)
+        return dot(left, jnp.concatenate([w[:, columns] for w in weights[4:6]], axis=0))
 
     for half, targets in enumerate((near_out, far_out)):
         rows = slice(half * near, (half + 1) * near)
@@ -203,11 +205,15 @@
         put_all(back_ref, me_ref[0], half * near, rest)
 
 
-def partial_kernel(count, experts, cap, me_ref, packet_ref, *refs):
-    masks = weighted(packet_ref[...], me_ref[0], experts, cap)
+def masks_kernel(experts, cap, me_ref, packet_ref, high_ref, low_ref):
+    high_ref[...], low_ref[...] = weighted(packet_ref[...], me_ref[0], experts, cap)
+
+
+def partial_kernel(count, high_ref, low_ref, *refs):
     segments, out_ref, rows_ref = refs[:count], refs[count], refs[count + 1]
     gather(segments, rows_ref)
-    out_ref[...] = sum(dot(mask, rows_ref[...]) for mask in masks).astype(BF16)
+    rows = rows_ref[...]
+    out_ref[...] = (dot(high_ref[...], rows) + dot(low_ref[...], rows)).astype(BF16)
 
 
 def shared_kernel(waits, normed_ref, *refs):
@@ -350,9 +356,17 @@
             me,
             other_packet,
             block,
+            resident=1,
             flops=near * rows * width,
         )
         other_in += exchange(other)
+    masks = call(
+        functools.partial(masks_kernel, half, cap),
+        [array((rows, near))] * 2,
+        me,
+        other_packet,
+        flops=rows * rows * near,
+    )
     *done, plain_out = call(
         functools.partial(ffn_kernel, count),
         [array((part, width))] * (2 * count) + [array(plain_shape)],
@@ -369,10 +383,9 @@
     other_back = exchange(done[count:])
     own_back = exchange(done[:count])
     (partial,) = call(
-        functools.partial(partial_kernel, count, half, cap),
+        functools.partial(partial_kernel, count),
         [array((rows, width))],
-        me,
-        other_packet,
+        *masks,
         *other_back,
         scratch=[pltpu.VMEM((near, width), BF16)],
         flops=4 * near * rows * width,
@@ -396,8 +409,16 @@
         shared_out,
         scratch=[pltpu.VMEM((near, width), BF16), pltpu.VMEM((2 * near, rest), BF16)],
         flops=4 * near * rows * (model_width + rest),
-    )
-    (out,) = call(last_kernel, [array((rows, model_width))], mine, passed, flops=rows * model_width)
+        keep=1,
+    )
+    (out,) = call(
+        last_kernel,
+        [array((rows, model_width))],
+        mine,
+        passed,
+        resident=2,
+        flops=rows * model_width,
+    )
     return out
 
 

time: 214 us -> 210 us (0.981)
  Pallas kernels: 40.5 us -> 38.2 us
    ppermute x39, starting transfers between devices: 57.2 us -> 54.5 us  [swap(): return lax.ppermute(array, 'ep', [(i, i ^ bits) for i in range(size)])]
    pallas_call x9 -> x10, Pallas kernels: 40.5 us -> 38.2 us  [call(): pl.pallas_call(wrapped, out_shape=tuple([space(o.shape, o.dtype) for o, s...]
    unnamed x116 -> x108, local copies, waits for them, and re-layouts: 5.92 us -> 5.21 us
  transfers between devices with their start and end apart: 47 -> 47, of which waited for: 28 -> 27; matrix products, arithmetic and copies ran while one was open for 0% -> 0% of each run, Pallas kernels for 10% -> 10%
where the time goes in v1:
time: 210 us
  waiting for transfers between devices  94.4 us (45%)
  starting transfers between devices  69.3 us (33%)
  Pallas kernels  38.2 us (18%)
  local copies, waits for them, and re-layouts  5.21 us (2%)
    ppermute x39, waiting for transfers between devices, swap(): return lax.ppermute(array, 'ep', [(i, i ^ bits) for i in range(size)])  94.4 us
    ppermute x39, starting transfers between devices, swap(): return lax.ppermute(array, 'ep', [(i, i ^ bits) for i in range(size)])  54.5 us
    pallas_call x10, Pallas kernels, call(): pl.pallas_call(wrapped, out_shape=tuple([space(o.shape, o.dtype) for o, s...  38.2 us
    all_to_all x2, starting transfers between devices, exchange_all(): blocks = lax.all_to_all(blocks, 'ep', 0, 0, tiled=True)  13.7 us
    unnamed x108, local copies, waits for them, and re-layouts  5.21 us
  transfers between devices with their start and end apart: 47, of which 27 were waited for; matrix products, arithmetic and copies ran while one was open for 0% of the time, Pallas kernels for 10%

profile of v1, /device:TPU:4, one launch (start us, length us, event | category | flops | bytes accessed | tf_op | source)
XLA Modules:
  0.0 209.9 jit_solution(1469772740872121941)
XLA Ops:
  0.7 3.0 %shard_map.100 = (bf16[256,2048]{1,0:T(8,128)(2,1)}, bf16[256,768]{1,0:T(8,128)(2,1)}, bf16[256,768]{1,0:T(8,128)(2,1)}) custom-call(bf16[256,2048]{1,0:T(8,128)(2,1)} %refs_0_.1, f32[1,2048]{1,0:T(1,128)} %bitcast.8), custom_call_target="tpu_custom_call" | custom-call | flops 2097152 | bytes 2891776 | tf_op jit(solution)/shard_map/pallas_call | solution.py:62
  5.0 3.5 %shard_map.101 = (bf16[48,1536]{1,0:T(8,128)(2,1)}, bf16[48,1536]{1,0:T(8,128)(2,1)}, bf16[48,1536]{1,0:T(8,128)(2,1)}, bf16[48,1536]{1,0:T(8,128)(2,1)}, bf16[4...) custom-call(s32[1]{0:T(128)} %bitcast.refs_0_, ...), custom_call_target="tpu_custom_call" | custom-call | flops 503316480 | bytes 3018756 | tf_op jit(solution)/shard_map/pallas_call | solution.py:62
  8.6 7.3 %all-to-all-start = ((bf16[16,48,512]{2,1,0:T(8,128)(2,1)}), bf16[16,48,512]{2,1,0:T(8,128)(2,1)S(1)}, u32[]{:S(2)}, u32[]{:S(2)}) async-start(bf16[16,48,512]{2,1,0:T(8,128)(2,1)} %get-tuple-element.79), calls=%async_computation | async-start | bytes 1572864 | tf_op jit(solution)/shard_map/all_to_all | solution.py:282
  17.9 2.4 %collective-permute-start.7 = (f32[4,256]{1,0:T(4,128)S(1)}, f32[4,256]{1,0:T(4,128)S(1)}, u32[]{:S(2)}, u32[]{:S(2)}) collective-permute-start(f32[4,256]{1,0:T(4,128)S(1)} %copy-done.20), channel_id=1, source_target_pairs={{0,16},{2,18},{4,20},{6,22},{8,24},{10,26},{12,28},{14,30},{16,0},... | collective-permute-start | bytes 12296 | tf_op jit(solution)/shard_map/ppermute | solution.py:261
  23.2 12.4 %collective-permute-done.7.refs_1_ = f32[4,256]{1,0:T(4,128)S(1)} collective-permute-done((f32[4,256]{1,0:T(4,128)S(1)}, f32[4,256]{1,0:T(4,128)S(1)}, u32[]{:S(2)}, u32[]{:S(2)}) %collective-permute-start.7) | collective-permute-done | bytes 4128 | tf_op jit(solution)/shard_map/ppermute | solution.py:261
  35.6 2.9 %collective-permute-start.8 = (bf16[256,768]{1,0:T(8,128)(2,1)}, bf16[256,768]{1,0:T(8,128)(2,1)S(1)}, u32[]{:S(2)}, u32[]{:S(2)}) collective-permute-start(bf16[256,768]{1,0:T(8,128)(2,1)} %get-tuple-element.61), channel_id=1, source_target_pairs={{0,16},{2,18},{4,20},{6,22},{8,24},{10,26},{12,28},{14,30},{16,0},... | collective-permute-start | bytes 1179656 | tf_op jit(solution)/shard_map/ppermute | solution.py:261
  40.4 4.6 %collective-permute-done.4.refs_6_ = bf16[48,1536]{1,0:T(8,128)(2,1)S(1)} collective-permute-done((bf16[48,1536]{1,0:T(8,128)(2,1)}, bf16[48,1536]{1,0:T(8,128)(2,1)S(1)}, u32[]{:S(2)}, u32[]{:S(2)}) %collective-permute-start.4) | collective-permute-done | bytes 147488 | tf_op jit(solution)/shard_map/ppermute | solution.py:261
  45.0 5.3 %collective-permute-done.5.refs_7_ = bf16[48,1536]{1,0:T(8,128)(2,1)S(1)} collective-permute-done((bf16[48,1536]{1,0:T(8,128)(2,1)}, bf16[48,1536]{1,0:T(8,128)(2,1)S(1)}, u32[]{:S(2)}, u32[]{:S(2)}) %collective-permute-start.5) | collective-permute-done | bytes 147488 | tf_op jit(solution)/shard_map/ppermute | solution.py:261
  50.2 2.9 %collective-permute-start.16 = (bf16[256,768]{1,0:T(8,128)(2,1)S(1)}, bf16[256,768]{1,0:T(8,128)(2,1)S(1)}, u32[]{:S(2)}, u32[]{:S(2)}) collective-permute-start(bf16[256,768]{1,0:T(8,128)(2,1)S(1)} %copy-done.24), channel_id=1, source_target_pairs={{0,16},{2,18},{4,20},{6,22},{8,24},{10,26},{12,28},{14,30},{16,0},... | collective-permute-start | bytes 1179656 | tf_op jit(solution)/shard_map/ppermute | solution.py:261
  53.1 12.5 %collective-permute-done.8.refs_2_ = bf16[256,768]{1,0:T(8,128)(2,1)S(1)} collective-permute-done((bf16[256,768]{1,0:T(8,128)(2,1)}, bf16[256,768]{1,0:T(8,128)(2,1)S(1)}, u32[]{:S(2)}, u32[]{:S(2)}) %collective-permute-start.8) | collective-permute-done | bytes 393248 | tf_op jit(solution)/shard_map/ppermute | solution.py:261
  67.9 6.7 %collective-permute-done.6.refs_8_ = bf16[48,1536]{1,0:T(8,128)(2,1)S(1)} collective-permute-done((bf16[48,1536]{1,0:T(8,128)(2,1)}, bf16[48,1536]{1,0:T(8,128)(2,1)S(1)}, u32[]{:S(2)}, u32[]{:S(2)}) %collective-permute-start.6) | collective-permute-done | bytes 147488 | tf_op jit(solution)/shard_map/ppermute | solution.py:261
  76.8 2.3 %collective-permute-done.10.refs_11_ = bf16[48,768]{1,0:T(8,128)(2,1)S(1)} collective-permute-done((bf16[48,768]{1,0:T(8,128)(2,1)}, bf16[48,768]{1,0:T(8,128)(2,1)S(1)}, u32[]{:S(2)}, u32[]{:S(2)}) %collective-permute-start.10) | collective-permute-done | bytes 73760 | tf_op jit(solution)/shard_map/ppermute | solution.py:261
  79.1 2.6 %collective-permute-done.11.refs_12_ = bf16[48,768]{1,0:T(8,128)(2,1)S(1)} collective-permute-done((bf16[48,768]{1,0:T(8,128)(2,1)}, bf16[48,768]{1,0:T(8,128)(2,1)S(1)}, u32[]{:S(2)}, u32[]{:S(2)}) %collective-permute-start.11) | collective-permute-done | bytes 73760 | tf_op jit(solution)/shard_map/ppermute | solution.py:261
  91.3 2.8 %collective-permute-done.15.refs_16_ = bf16[48,768]{1,0:T(8,128)(2,1)S(1)} collective-permute-done((bf16[48,768]{1,0:T(8,128)(2,1)}, bf16[48,768]{1,0:T(8,128)(2,1)S(1)}, u32[]{:S(2)}, u32[]{:S(2)}) %collective-permute-start.15) | collective-permute-done | bytes 73760 | tf_op jit(solution)/shard_map/ppermute | solution.py:261
  94.9 2.7 %collective-permute-start.19 = (bf16[48,768]{1,0:T(8,128)(2,1)}, bf16[48,768]{1,0:T(8,128)(2,1)S(1)}, u32[]{:S(2)}, u32[]{:S(2)}) collective-permute-start(bf16[48,768]{1,0:T(8,128)(2,1)} %get-tuple-element.74), channel_id=1, source_target_pairs={{0,6},{2,4},{4,2},{6,0},{8,14},{10,12},{12,10},{14,8},{16,22},{18,... | collective-permute-start | bytes 221192 | tf_op jit(solution)/shard_map/ppermute | solution.py:261
  100.5 3.9 %collective-permute-start.21 = (bf16[48,768]{1,0:T(8,128)(2,1)}, bf16[48,768]{1,0:T(8,128)(2,1)S(1)}, u32[]{:S(2)}, u32[]{:S(2)}) collective-permute-start(bf16[48,768]{1,0:T(8,128)(2,1)} %get-tuple-element.76), channel_id=1, source_target_pairs={{0,10},{2,8},{4,14},{6,12},{8,2},{10,0},{12,6},{14,4},{16,26},{18,... | collective-permute-start | bytes 221192 | tf_op jit(solution)/shard_map/ppermute | solution.py:261
  107.0 3.2 %collective-permute-start.23 = (bf16[48,768]{1,0:T(8,128)(2,1)}, bf16[48,768]{1,0:T(8,128)(2,1)S(1)}, u32[]{:S(2)}, u32[]{:S(2)}) collective-permute-start(bf16[48,768]{1,0:T(8,128)(2,1)} %get-tuple-element.78), channel_id=1, source_target_pairs={{0,14},{2,12},{4,10},{6,8},{8,6},{10,4},{12,2},{14,0},{16,30},{18,... | collective-permute-start | bytes 221192 | tf_op jit(solution)/shard_map/ppermute | solution.py:261
  111.0 2.3 %collective-permute-done.23.refs_24_ = bf16[48,768]{1,0:T(8,128)(2,1)S(1)} collective-permute-done((bf16[48,768]{1,0:T(8,128)(2,1)}, bf16[48,768]{1,0:T(8,128)(2,1)S(1)}, u32[]{:S(2)}, u32[]{:S(2)}) %collective-permute-start.23) | collective-permute-done | bytes 73760 | tf_op jit(solution)/shard_map/ppermute | solution.py:261
  117.3 9.6 %shard_map.104 = (bf16[48,1536]{1,0:T(8,128)(2,1)}, bf16[48,1536]{1,0:T(8,128)(2,1)}, bf16[48,1536]{1,0:T(8,128)(2,1)}, bf16[48,1536]{1,0:T(8,128)(2,1)}, bf16[4...) custom-call(s32[1]{0:T(128)} %bitcast.refs_0_, ...), custom_call_target="tpu_custom_call" | custom-call | flops 4831838208 | bytes 12582916 | tf_op jit(solution)/shard_map/pallas_call | solution.py:62
  127.0 6.4 %all-to-all-start.1 = ((bf16[16,48,512]{2,1,0:T(8,128)(2,1)}), bf16[16,48,512]{2,1,0:T(8,128)(2,1)S(1)}, u32[]{:S(2)}, u32[]{:S(2)}) async-start(bf16[16,48,512]{2,1,0:T(8,128)(2,1)} %get-tuple-element.88), calls=%async_computation.1 | async-start | bytes 1572864 | tf_op jit(solution)/shard_map/all_to_all | solution.py:282
  136.1 7.3 %collective-permute-done.37.refs_3_ = bf16[48,1536]{1,0:T(8,128)(2,1)S(1)} collective-permute-done((bf16[48,1536]{1,0:T(8,128)(2,1)}, bf16[48,1536]{1,0:T(8,128)(2,1)S(1)}, u32[]{:S(2)}, u32[]{:S(2)}) %collective-permute-start.37) | collective-permute-done | bytes 147488 | tf_op jit(solution)/shard_map/ppermute | solution.py:261
  146.1 3.6 %collective-permute-done.39.refs_5_ = bf16[48,1536]{1,0:T(8,128)(2,1)S(1)} collective-permute-done((bf16[48,1536]{1,0:T(8,128)(2,1)}, bf16[48,1536]{1,0:T(8,128)(2,1)S(1)}, u32[]{:S(2)}, u32[]{:S(2)}) %collective-permute-start.39) | collective-permute-done | bytes 147488 | tf_op jit(solution)/shard_map/ppermute | solution.py:261
  152.3 4.1 %collective-permute-done.41.refs_7_ = bf16[48,1536]{1,0:T(8,128)(2,1)S(1)} collective-permute-done((bf16[48,1536]{1,0:T(8,128)(2,1)}, bf16[48,1536]{1,0:T(8,128)(2,1)S(1)}, u32[]{:S(2)}, u32[]{:S(2)}) %collective-permute-start.41) | collective-permute-done | bytes 147488 | tf_op jit(solution)/shard_map/ppermute | solution.py:261
  158.3 2.2 %shard_map.107 = (bf16[256,384]{1,0:T(8,128)(2,1)}, bf16[256,384]{1,0:T(8,128)(2,1)}) custom-call(s32[1]{0:T(128)} %bitcast.refs_0_, f32[4,256]{1,0:T(4,128)} %copy-done.53), custom_call_target="tpu_custom_call" | custom-call | flops 25165824 | bytes 397316 | tf_op jit(solution)/shard_map/pallas_call | solution.py:62
  160.5 3.0 %collective-permute-done.43.refs_9_ = bf16[48,1536]{1,0:T(8,128)(2,1)S(1)} collective-permute-done((bf16[48,1536]{1,0:T(8,128)(2,1)}, bf16[48,1536]{1,0:T(8,128)(2,1)S(1)}, u32[]{:S(2)}, u32[]{:S(2)}) %collective-permute-start.43) | collective-permute-done | bytes 147488 | tf_op jit(solution)/shard_map/ppermute | solution.py:261
  164.2 3.4 %shard_map.108 = bf16[256,1536]{1,0:T(8,128)(2,1)} custom-call(bf16[256,384]{1,0:T(8,128)(2,1)} %get-tuple-element.89.refs_0_, bf16[256,384]{1,0:T(8,128)(2,1)} %get-tuple-element.90.refs_1_, bf16[48,1536]{1,0:T(8,128)(2,1)} %get-tuple-element.91.refs_2_, bf16[48,1536]{1,0:T(8,128)(2,1)} %copy-done.9, bf16[48,1536]{1,0:T(8,128)(2,1)} %copy-done.11, ...), custom_call_target="tpu_custom_call" | custom-call | flops 603979776 | bytes 2359296 | tf_op jit(solution)/shard_map/pallas_call | solution.py:62
  176.4 3.4 %collective-permute-start.32 = (bf16[48,1536]{1,0:T(8,128)(2,1)S(1)}, bf16[48,1536]{1,0:T(8,128)(2,1)S(1)}, u32[]{:S(2)}, u32[]{:S(2)}) collective-permute-start(bf16[48,1536]{1,0:T(8,128)(2,1)S(1)} %copy-done.32), channel_id=1, source_target_pairs={{0,12},{2,14},{4,8},{6,10},{8,4},{10,6},{12,0},{14,2},{16,28},{18,... | collective-permute-start | bytes 442376 | tf_op jit(solution)/shard_map/ppermute | solution.py:261
  180.0 4.1 %collective-permute-start.33 = (bf16[48,1536]{1,0:T(8,128)(2,1)S(1)}, bf16[48,1536]{1,0:T(8,128)(2,1)S(1)}, u32[]{:S(2)}, u32[]{:S(2)}) collective-permute-start(bf16[48,1536]{1,0:T(8,128)(2,1)S(1)} %copy-done.31), channel_id=1, source_target_pairs={{0,14},{2,12},{4,10},{6,8},{8,6},{10,4},{12,2},{14,0},{16,30},{18,... | collective-permute-start | bytes 442376 | tf_op jit(solution)/shard_map/ppermute | solution.py:261
  184.1 6.4 %shard_map.105.refs_11_ = f32[256,2048]{1,0:T(8,128)} custom-call(bf16[256,2048]{1,0:T(8,128)(2,1)} %get-tuple-element.52.refs_2_.refs_0_, bf16[2048,256]{1,0:T(8,128)(2,1)} %refs_1_.1, bf16[2048,256]{1,0:T(8,128)(2,1)} %refs_2_.1, bf16[2048,256]{1,0:T(8,128)(2,1)} %copy-done.2, bf16[2048,256]{1,0:T(8,128)(2,1)} %copy-done.3, bf16[256,2048]{1,0:T(8,128)(2,1)} %refs_5_.1, ...), custom_call_target="tpu_custom_call" | custom-call | flops 1610612736 | bytes 9437184 | tf_op jit(solution)/shard_map/pallas_call | solution.py:62
  191.0 2.3 %collective-permute-done.31.refs_7_ = bf16[48,1536]{1,0:T(8,128)(2,1)S(1)} collective-permute-done((bf16[48,1536]{1,0:T(8,128)(2,1)S(1)}, bf16[48,1536]{1,0:T(8,128)(2,1)S(1)}, u32[]{:S(2)}, u32[]{:S(2)}) %collective-permute-start.31) | collective-permute-done | bytes 147488 | tf_op jit(solution)/shard_map/ppermute | solution.py:261
  194.8 8.1 %collective-permute-done.33.refs_9_ = bf16[48,1536]{1,0:T(8,128)(2,1)S(1)} collective-permute-done((bf16[48,1536]{1,0:T(8,128)(2,1)S(1)}, bf16[48,1536]{1,0:T(8,128)(2,1)S(1)}, u32[]{:S(2)}, u32[]{:S(2)}) %collective-permute-start.33) | collective-permute-done | bytes 147488 | tf_op jit(solution)/shard_map/ppermute | solution.py:261
  203.9 4.6 %shard_map.106.refs_0_ = f32[256,2048]{1,0:T(8,128)S(1)} custom-call(s32[1]{0:T(128)} %bitcast.refs_0_, f32[4,256]{1,0:T(4,128)} %pad_maximum_fusion.refs_1_, bf16[48,1536]{1,0:T(8,128)(2,1)} %get-tuple-element.80.refs_2_, bf16[48,1536]{1,0:T(8,128)(2,1)} %copy-done.6, bf16[48,1536]{1,0:T(8,128)(2,1)} %copy-done.7, bf16[48,1536]{1,0:T(8,128)(2,1)} %copy-done.8, ...), custom_call_target="tpu_custom_call" | custom-call | flops 1006632960 | bytes 6164484 | tf_op jit(solution)/shard_map/pallas_call | solution.py:62
  (182 shorter events, 57.3 us)
Async XLA Ops:
  8.6 107.9 %all-to-all-start = ((bf16[16,48,512]{2,1,0:T(8,128)(2,1)}), bf16[16,48,512]{2,1,0:T(8,128)(2,1)S(1)}, u32[]{:S(2)}, u32[]{:S(2)}) async-start(bf16[16,48,512]{2,1,0:T(8,128)(2,1)} %get-tuple-element.79), calls=%async_computation | async-start | bytes 1572864 | tf_op jit(solution)/shard_map/all_to_all | solution.py:282
  15.9 19.8 %collective-permute-start = (bf16[48,1536]{1,0:T(8,128)(2,1)}, bf16[48,1536]{1,0:T(8,128)(2,1)S(1)}, u32[]{:S(2)}, u32[]{:S(2)}) collective-permute-start(bf16[48,1536]{1,0:T(8,128)(2,1)} %get-tuple-element.54), channel_id=1, source_target_pairs={{0,2},{2,0},{4,6},{6,4},{8,10},{10,8},{12,14},{14,12},{16,18},{18,... | collective-permute-start | bytes 442376 | tf_op jit(solution)/shard_map/ppermute | solution.py:261
  17.3 21.2 %collective-permute-start.1 = (bf16[48,1536]{1,0:T(8,128)(2,1)}, bf16[48,1536]{1,0:T(8,128)(2,1)S(1)}, u32[]{:S(2)}, u32[]{:S(2)}) collective-permute-start(bf16[48,1536]{1,0:T(8,128)(2,1)} %get-tuple-element.55), channel_id=1, source_target_pairs={{0,4},{2,6},{4,0},{6,2},{8,12},{10,14},{12,8},{14,10},{16,20},{18,... | collective-permute-start | bytes 442376 | tf_op jit(solution)/shard_map/ppermute | solution.py:261
  17.9 17.7 %collective-permute-start.7 = (f32[4,256]{1,0:T(4,128)S(1)}, f32[4,256]{1,0:T(4,128)S(1)}, u32[]{:S(2)}, u32[]{:S(2)}) collective-permute-start(f32[4,256]{1,0:T(4,128)S(1)} %copy-done.20), channel_id=1, source_target_pairs={{0,16},{2,18},{4,20},{6,22},{8,24},{10,26},{12,28},{14,30},{16,0},... | collective-permute-start | bytes 12296 | tf_op jit(solution)/shard_map/ppermute | solution.py:261
  20.2 18.4 %collective-permute-start.2 = (bf16[48,1536]{1,0:T(8,128)(2,1)}, bf16[48,1536]{1,0:T(8,128)(2,1)S(1)}, u32[]{:S(2)}, u32[]{:S(2)}) collective-permute-start(bf16[48,1536]{1,0:T(8,128)(2,1)} %get-tuple-element.56), channel_id=1, source_target_pairs={{0,6},{2,4},{4,2},{6,0},{8,14},{10,12},{12,10},{14,8},{16,22},{18,... | collective-permute-start | bytes 442376 | tf_op jit(solution)/shard_map/ppermute | solution.py:261
  21.7 18.1 %collective-permute-start.3 = (bf16[48,1536]{1,0:T(8,128)(2,1)}, bf16[48,1536]{1,0:T(8,128)(2,1)S(1)}, u32[]{:S(2)}, u32[]{:S(2)}) collective-permute-start(bf16[48,1536]{1,0:T(8,128)(2,1)} %get-tuple-element.57), channel_id=1, source_target_pairs={{0,8},{2,10},{4,12},{6,14},{8,0},{10,2},{12,4},{14,6},{16,24},{18,... | collective-permute-start | bytes 442376 | tf_op jit(solution)/shard_map/ppermute | solution.py:261
  35.6 9.3 %collective-permute-start.4 = (bf16[48,1536]{1,0:T(8,128)(2,1)}, bf16[48,1536]{1,0:T(8,128)(2,1)S(1)}, u32[]{:S(2)}, u32[]{:S(2)}) collective-permute-start(bf16[48,1536]{1,0:T(8,128)(2,1)} %get-tuple-element.58), channel_id=1, source_target_pairs={{0,10},{2,8},{4,14},{6,12},{8,2},{10,0},{12,6},{14,4},{16,26},{18,... | collective-permute-start | bytes 442376 | tf_op jit(solution)/shard_map/ppermute | solution.py:261
  35.6 30.0 %collective-permute-start.8 = (bf16[256,768]{1,0:T(8,128)(2,1)}, bf16[256,768]{1,0:T(8,128)(2,1)S(1)}, u32[]{:S(2)}, u32[]{:S(2)}) collective-permute-start(bf16[256,768]{1,0:T(8,128)(2,1)} %get-tuple-element.61), channel_id=1, source_target_pairs={{0,16},{2,18},{4,20},{6,22},{8,24},{10,26},{12,28},{14,30},{16,0},... | collective-permute-start | bytes 1179656 | tf_op jit(solution)/shard_map/ppermute | solution.py:261
  38.5 11.7 %collective-permute-start.5 = (bf16[48,1536]{1,0:T(8,128)(2,1)}, bf16[48,1536]{1,0:T(8,128)(2,1)S(1)}, u32[]{:S(2)}, u32[]{:S(2)}) collective-permute-start(bf16[48,1536]{1,0:T(8,128)(2,1)} %get-tuple-element.59), channel_id=1, source_target_pairs={{0,12},{2,14},{4,8},{6,10},{8,4},{10,6},{12,0},{14,2},{16,28},{18,... | collective-permute-start | bytes 442376 | tf_op jit(solution)/shard_map/ppermute | solution.py:261
  39.8 75.0 %collective-permute-start.24 = (bf16[2048,256]{1,0:T(8,128)(2,1)S(1)}, bf16[2048,256]{1,0:T(8,128)(2,1)S(1)}, u32[]{:S(2)}, u32[]{:S(2)}) collective-permute-start(bf16[2048,256]{1,0:T(8,128)(2,1)S(1)} %bitcast.11), channel_id=1, source_target_pairs={{0,1},{1,0},{2,3},{3,2},{4,5},{5,4},{6,7},{7,6},{8,9},{9,8},{10,11... | collective-permute-start | bytes 3145736 | tf_op jit(solution)/shard_map/ppermute | solution.py:256
  39.9 75.0 %collective-permute-start.25 = (bf16[2048,256]{1,0:T(8,128)(2,1)}, bf16[2048,256]{1,0:T(8,128)(2,1)S(1)}, u32[]{:S(2)}, u32[]{:S(2)}) collective-permute-start(bf16[2048,256]{1,0:T(8,128)(2,1)} %bitcast.12), channel_id=1, source_target_pairs={{0,1},{1,0},{2,3},{3,2},{4,5},{5,4},{6,7},{7,6},{8,9},{9,8},{10,11... | collective-permute-start | bytes 3145736 | tf_op jit(solution)/shard_map/ppermute | solution.py:256
  45.0 71.5 %collective-permute-start.26 = (bf16[256,2048]{1,0:T(8,128)(2,1)}, bf16[256,2048]{1,0:T(8,128)(2,1)}, u32[]{:S(2)}, u32[]{:S(2)}) collective-permute-start(bf16[256,2048]{1,0:T(8,128)(2,1)} %bitcast.14), channel_id=1, source_target_pairs={{0,1},{1,0},{2,3},{3,2},{4,5},{5,4},{6,7},{7,6},{8,9},{9,8},{10,11... | collective-permute-start | bytes 3145736 | tf_op jit(solution)/shard_map/ppermute | solution.py:256
  50.2 25.9 %collective-permute-start.16 = (bf16[256,768]{1,0:T(8,128)(2,1)S(1)}, bf16[256,768]{1,0:T(8,128)(2,1)S(1)}, u32[]{:S(2)}, u32[]{:S(2)}) collective-permute-start(bf16[256,768]{1,0:T(8,128)(2,1)S(1)} %copy-done.24), channel_id=1, source_target_pairs={{0,16},{2,18},{4,20},{6,22},{8,24},{10,26},{12,28},{14,30},{16,0},... | collective-permute-start | bytes 1179656 | tf_op jit(solution)/shard_map/ppermute | solution.py:261
  65.6 8.9 %collective-permute-start.6 = (bf16[48,1536]{1,0:T(8,128)(2,1)}, bf16[48,1536]{1,0:T(8,128)(2,1)S(1)}, u32[]{:S(2)}, u32[]{:S(2)}) collective-permute-start(bf16[48,1536]{1,0:T(8,128)(2,1)} %get-tuple-element.60), channel_id=1, source_target_pairs={{0,14},{2,12},{4,10},{6,8},{8,6},{10,4},{12,2},{14,0},{16,30},{18,... | collective-permute-start | bytes 442376 | tf_op jit(solution)/shard_map/ppermute | solution.py:261
  87.3 6.9 %collective-permute-start.15 = (bf16[48,768]{1,0:T(8,128)(2,1)}, bf16[48,768]{1,0:T(8,128)(2,1)S(1)}, u32[]{:S(2)}, u32[]{:S(2)}) collective-permute-start(bf16[48,768]{1,0:T(8,128)(2,1)} %get-tuple-element.69), channel_id=1, source_target_pairs={{0,14},{2,12},{4,10},{6,8},{8,6},{10,4},{12,2},{14,0},{16,30},{18,... | collective-permute-start | bytes 221192 | tf_op jit(solution)/shard_map/ppermute | solution.py:261
  127.0 75.9 %all-to-all-start.1 = ((bf16[16,48,512]{2,1,0:T(8,128)(2,1)}), bf16[16,48,512]{2,1,0:T(8,128)(2,1)S(1)}, u32[]{:S(2)}, u32[]{:S(2)}) async-start(bf16[16,48,512]{2,1,0:T(8,128)(2,1)} %get-tuple-element.88), calls=%async_computation.1 | async-start | bytes 1572864 | tf_op jit(solution)/shard_map/all_to_all | solution.py:282
  133.5 36.9 %collective-permute-start.34 = (bf16[2048,256]{1,0:T(8,128)(2,1)S(1)}, bf16[2048,256]{1,0:T(8,128)(2,1)S(1)}, u32[]{:S(2)}, u32[]{:S(2)}) collective-permute-start(bf16[2048,256]{1,0:T(8,128)(2,1)S(1)} %copy-done.1), channel_id=1, source_target_pairs={{0,1},{1,0},{2,3},{3,2},{4,5},{5,4},{6,7},{7,6},{8,9},{9,8},{10,11... | collective-permute-start | bytes 3145736 | tf_op jit(solution)/shard_map/ppermute | solution.py:256
  133.5 37.6 %collective-permute-start.35 = (bf16[2048,256]{1,0:T(8,128)(2,1)}, bf16[2048,256]{1,0:T(8,128)(2,1)S(1)}, u32[]{:S(2)}, u32[]{:S(2)}) collective-permute-start(bf16[2048,256]{1,0:T(8,128)(2,1)} %refs_2_.1), channel_id=1, source_target_pairs={{0,1},{1,0},{2,3},{3,2},{4,5},{5,4},{6,7},{7,6},{8,9},{9,8},{10,11... | collective-permute-start | bytes 3145736 | tf_op jit(solution)/shard_map/ppermute | solution.py:256
  134.0 9.4 %collective-permute-start.37 = (bf16[48,1536]{1,0:T(8,128)(2,1)}, bf16[48,1536]{1,0:T(8,128)(2,1)S(1)}, u32[]{:S(2)}, u32[]{:S(2)}) collective-permute-start(bf16[48,1536]{1,0:T(8,128)(2,1)} %get-tuple-element.92), channel_id=1, source_target_pairs={{0,2},{2,0},{4,6},{6,4},{8,10},{10,8},{12,14},{14,12},{16,18},{18,... | collective-permute-start | bytes 442376 | tf_op jit(solution)/shard_map/ppermute | solution.py:261
  135.5 37.8 %collective-permute-start.36 = (bf16[256,2048]{1,0:T(8,128)(2,1)}, bf16[256,2048]{1,0:T(8,128)(2,1)S(1)}, u32[]{:S(2)}, u32[]{:S(2)}) collective-permute-start(bf16[256,2048]{1,0:T(8,128)(2,1)} %refs_5_.1), channel_id=1, source_target_pairs={{0,1},{1,0},{2,3},{3,2},{4,5},{5,4},{6,7},{7,6},{8,9},{9,8},{10,11... | collective-permute-start | bytes 3145736 | tf_op jit(solution)/shard_map/ppermute | solution.py:256
  135.5 8.5 %collective-permute-start.38 = (bf16[48,1536]{1,0:T(8,128)(2,1)}, bf16[48,1536]{1,0:T(8,128)(2,1)S(1)}, u32[]{:S(2)}, u32[]{:S(2)}) collective-permute-start(bf16[48,1536]{1,0:T(8,128)(2,1)} %get-tuple-element.93), channel_id=1, source_target_pairs={{0,4},{2,6},{4,0},{6,2},{8,12},{10,14},{12,8},{14,10},{16,20},{18,... | collective-permute-start | bytes 442376 | tf_op jit(solution)/shard_map/ppermute | solution.py:261
  144.0 7.7 %collective-permute-start.40 = (bf16[48,1536]{1,0:T(8,128)(2,1)}, bf16[48,1536]{1,0:T(8,128)(2,1)S(1)}, u32[]{:S(2)}, u32[]{:S(2)}) collective-permute-start(bf16[48,1536]{1,0:T(8,128)(2,1)} %get-tuple-element.95), channel_id=1, source_target_pairs={{0,8},{2,10},{4,12},{6,14},{8,0},{10,2},{12,4},{14,6},{16,24},{18,... | collective-permute-start | bytes 442376 | tf_op jit(solution)/shard_map/ppermute | solution.py:261
  149.7 6.7 %collective-permute-start.41 = (bf16[48,1536]{1,0:T(8,128)(2,1)}, bf16[48,1536]{1,0:T(8,128)(2,1)S(1)}, u32[]{:S(2)}, u32[]{:S(2)}) collective-permute-start(bf16[48,1536]{1,0:T(8,128)(2,1)} %get-tuple-element.96), channel_id=1, source_target_pairs={{0,10},{2,8},{4,14},{6,12},{8,2},{10,0},{12,6},{14,4},{16,26},{18,... | collective-permute-start | bytes 442376 | tf_op jit(solution)/shard_map/ppermute | solution.py:261
  151.7 8.8 %collective-permute-start.42 = (bf16[48,1536]{1,0:T(8,128)(2,1)}, bf16[48,1536]{1,0:T(8,128)(2,1)S(1)}, u32[]{:S(2)}, u32[]{:S(2)}) collective-permute-start(bf16[48,1536]{1,0:T(8,128)(2,1)} %get-tuple-element.97), channel_id=1, source_target_pairs={{0,12},{2,14},{4,8},{6,10},{8,4},{10,6},{12,0},{14,2},{16,28},{18,... | collective-permute-start | bytes 442376 | tf_op jit(solution)/shard_map/ppermute | solution.py:261
  156.4 7.2 %collective-permute-start.43 = (bf16[48,1536]{1,0:T(8,128)(2,1)}, bf16[48,1536]{1,0:T(8,128)(2,1)S(1)}, u32[]{:S(2)}, u32[]{:S(2)}) collective-permute-start(bf16[48,1536]{1,0:T(8,128)(2,1)} %get-tuple-element.98), channel_id=1, source_target_pairs={{0,14},{2,12},{4,10},{6,8},{8,6},{10,4},{12,2},{14,0},{16,30},{18,... | collective-permute-start | bytes 442376 | tf_op jit(solution)/shard_map/ppermute | solution.py:261
  167.7 40.9 %collective-permute-start.44 = (bf16[256,1536]{1,0:T(8,128)(2,1)}, bf16[256,1536]{1,0:T(8,128)(2,1)S(1)}, u32[]{:S(2)}, u32[]{:S(2)}) collective-permute-start(bf16[256,1536]{1,0:T(8,128)(2,1)} %shard_map.108), channel_id=1, source_target_pairs={{0,16},{2,18},{4,20},{6,22},{8,24},{10,26},{12,28},{14,30},{16,0},... | collective-permute-start | bytes 2359304 | tf_op jit(solution)/shard_map/ppermute | solution.py:261
  169.6 6.7 %collective-permute-start.27 = (bf16[48,1536]{1,0:T(8,128)(2,1)S(1)}, bf16[48,1536]{1,0:T(8,128)(2,1)S(1)}, u32[]{:S(2)}, u32[]{:S(2)}) collective-permute-start(bf16[48,1536]{1,0:T(8,128)(2,1)S(1)} %copy-done.38), channel_id=1, source_target_pairs={{0,2},{2,0},{4,6},{6,4},{8,10},{10,8},{12,14},{14,12},{16,18},{18,... | collective-permute-start | bytes 442376 | tf_op jit(solution)/shard_map/ppermute | solution.py:261
  171.2 8.8 %collective-permute-start.29 = (bf16[48,1536]{1,0:T(8,128)(2,1)S(1)}, bf16[48,1536]{1,0:T(8,128)(2,1)S(1)}, u32[]{:S(2)}, u32[]{:S(2)}) collective-permute-start(bf16[48,1536]{1,0:T(8,128)(2,1)S(1)} %copy-done.36), channel_id=1, source_target_pairs={{0,6},{2,4},{4,2},{6,0},{8,14},{10,12},{12,10},{14,8},{16,22},{18,... | collective-permute-start | bytes 442376 | tf_op jit(solution)/shard_map/ppermute | solution.py:261
  173.3 17.7 %collective-permute-start.30 = (bf16[48,1536]{1,0:T(8,128)(2,1)S(1)}, bf16[48,1536]{1,0:T(8,128)(2,1)S(1)}, u32[]{:S(2)}, u32[]{:S(2)}) collective-permute-start(bf16[48,1536]{1,0:T(8,128)(2,1)S(1)} %copy-done.35), channel_id=1, source_target_pairs={{0,8},{2,10},{4,12},{6,14},{8,0},{10,2},{12,4},{14,6},{16,24},{18,... | collective-permute-start | bytes 442376 | tf_op jit(solution)/shard_map/ppermute | solution.py:261
  176.4 16.9 %collective-permute-start.31 = (bf16[48,1536]{1,0:T(8,128)(2,1)S(1)}, bf16[48,1536]{1,0:T(8,128)(2,1)S(1)}, u32[]{:S(2)}, u32[]{:S(2)}) collective-permute-start(bf16[48,1536]{1,0:T(8,128)(2,1)S(1)} %copy-done.34), channel_id=1, source_target_pairs={{0,10},{2,8},{4,14},{6,12},{8,2},{10,0},{12,6},{14,4},{16,26},{18,... | collective-permute-start | bytes 442376 | tf_op jit(solution)/shard_map/ppermute | solution.py:261
  176.4 18.4 %collective-permute-start.32 = (bf16[48,1536]{1,0:T(8,128)(2,1)S(1)}, bf16[48,1536]{1,0:T(8,128)(2,1)S(1)}, u32[]{:S(2)}, u32[]{:S(2)}) collective-permute-start(bf16[48,1536]{1,0:T(8,128)(2,1)S(1)} %copy-done.32), channel_id=1, source_target_pairs={{0,12},{2,14},{4,8},{6,10},{8,4},{10,6},{12,0},{14,2},{16,28},{18,... | collective-permute-start | bytes 442376 | tf_op jit(solution)/shard_map/ppermute | solution.py:261
  180.0 22.9 %collective-permute-start.33 = (bf16[48,1536]{1,0:T(8,128)(2,1)S(1)}, bf16[48,1536]{1,0:T(8,128)(2,1)S(1)}, u32[]{:S(2)}, u32[]{:S(2)}) collective-permute-start(bf16[48,1536]{1,0:T(8,128)(2,1)S(1)} %copy-done.31), channel_id=1, source_target_pairs={{0,14},{2,12},{4,10},{6,8},{8,6},{10,4},{12,2},{14,0},{16,30},{18,... | collective-permute-start | bytes 442376 | tf_op jit(solution)/shard_map/ppermute | solution.py:261
  (69 other events, 1173.4 us)
